TPU v7x, 1024 devices: a whole 4x4x32 slice. The times are simulated.
1024 devices in a mesh: sp: 64 (over z, core), tp: 16 (over y, x).
Axes of the slice: x: 4, y: 4, z: 32, core: 2. Of those that a mesh axis runs over, the one named last changes fastest.
Arguments:
- tokens: bfloat16 [16384, 4096], P('sp'), may hold values from -6 to 6
- norm_gain: float32 [2, 4096], replicated, may hold values from 0.1 to 1.9
- w_outer: bfloat16 [2, 4096, 1024], P(None, 'sp', 'tp'), may hold values from -0.09375 to 0.09375
- w_inner: bfloat16 [2, 4096, 1024], P(None, 'sp', 'tp'), may hold values from -0.09375 to 0.09375
- w_value: bfloat16 [2, 4096, 1024], P(None, 'sp', 'tp'), may hold values from -0.09375 to 0.09375
- w_back: bfloat16 [2, 1024, 4096], P(None, 'sp', 'tp'), may hold values from -0.1875 to 0.1875
- taps: float32 [2, 3, 1024], P(None, None, 'tp'), may hold values from -3 to 3
Outputs:
- result: bfloat16 [16384, 4096], P('sp', 'tp')
All inputs are finite; a program needn't handle non-finite values.
Results may differ from a plain program's by a relative error of at most 0.022.
Values may be sent and summed in bfloat16 or wider, within the bound.
No kernel may reach another device: no remote copies, remote signals or barrier semaphores. Data moves between devices by JAX's collectives and lax.ppermute only.
A program may use at most 32 MiB of HBM per device.

v0:
```python
import jax
import jax.numpy as jnp
from jax import lax
from jax.sharding import PartitionSpec as P

eps = 1e-06


def in_order(parts, dim):
    parts = jnp.moveaxis(parts, 0, dim)
    lengths = parts.shape
    return parts.reshape(*lengths[:dim], lengths[dim] * lengths[dim + 1], *lengths[dim + 2 :])


def gather_packed(arrays, axis, dims):
    ravelled = jnp.concatenate([a.reshape(-1) for a in arrays])
    lines, at, finished = (lax.all_gather(ravelled, axis), 0, [])
    for a, dim in zip(arrays, dims):
        parts = lines[:, at : at + a.size].reshape(-1, *a.shape)
        finished.append(in_order(parts, dim))
        at += a.size
    return tuple(finished)


def copy_for_each(array, axis):
    length = lax.axis_size(axis)
    return lax.all_to_all(
        jnp.broadcast_to(array[None], (length, *array.shape)), axis, 0, 0, tiled=True
    )


def gather_directly(array, axis, dim):
    return in_order(copy_for_each(array, axis), dim)


def shifted(block, axis, distance):
    devices = range(lax.axis_size(axis))
    route = [(i - distance, i) for i in devices if i - distance in devices]
    return lax.ppermute(block, axis, route)


def per_device(tokens, norm_gain, w_outer, w_inner, w_value, w_back, taps):
    layers = w_outer.shape[0]
    count = tokens.shape[0]
    feats = w_back.shape[2]
    own = lax.axis_index("tp")
    held = gather_packed((w_outer, w_inner, w_value, w_back), "sp", (1, 1, 1, 1))
    current = tokens
    resid = lax.dynamic_slice_in_dim(tokens, own * feats, feats, 1)
    for layer in range(layers):
        if layer > 0:
            current = gather_directly(resid, "tp", 1)
        xf = current.astype(jnp.float32)
        normed = (
            xf * lax.rsqrt(jnp.mean(xf * xf, axis=-1, keepdims=True) + eps) * norm_gain[layer]
        ).astype(jnp.bfloat16)
        outer = jnp.dot(normed, held[0][layer], preferred_element_type=jnp.float32)
        inner = jnp.dot(normed, held[1][layer], preferred_element_type=jnp.float32)
        value = jnp.dot(normed, held[2][layer], preferred_element_type=jnp.float32)
        outer = outer.astype(jnp.bfloat16)
        inner = inner.astype(jnp.bfloat16)
        value = value.astype(jnp.bfloat16)
        mixed = (inner.astype(jnp.float32) * value.astype(jnp.float32)).astype(jnp.bfloat16)
        before = shifted(mixed[count - 2 :], "sp", 1)
        padded = jnp.concatenate([before, mixed], axis=0).astype(jnp.float32)
        conv = (
            taps[layer, 0] * padded[:count]
            + taps[layer, 1] * padded[1 : count + 1]
            + taps[layer, 2] * padded[2:]
        )
        gated = (outer.astype(jnp.float32) * conv).astype(jnp.bfloat16)
        whole = gather_directly(gated, "tp", 1)
        proj = jnp.dot(whole, held[3][layer], preferred_element_type=jnp.float32)
        resid = (resid.astype(jnp.float32) + proj).astype(jnp.bfloat16)
    return resid


def solution(mesh):
    in_specs = (
        P("sp", None),
        P(),
        P(None, "sp", "tp"),
        P(None, "sp", "tp"),
        P(None, "sp", "tp"),
        P(None, "sp", "tp"),
        P(None, None, "tp"),
    )
    out_specs = P("sp", "tp")
    return jax.shard_map(
        per_device, mesh=mesh, in_specs=in_specs, out_specs=out_specs, check_vma=False
    )
```

profile of v0, /device:TPU:32, one launch (start us, length us, event | category | flops | bytes accessed | tf_op | source)
XLA Modules:
  0.0 277.5 jit_solution(13140767295370399801)
XLA Ops:
  10.5 2.1 fusion
  12.7 142.7 %all-gather.3.cloned.1.call-done = bf16[2097152]{0:T(1024)(128)(2,1)} async-done(((bf16[32768]{0:T(1024)(128)(2,1)}), bf16[2097152]{0:T(1024)(128)(2,1)}) %all-gather.3.cloned.1.call-update) | async-done | bytes 4194320 | tf_op jit(solution)/shard_map/all_gather | solution.py:17
  155.4 7.3 %reshape.119 = bf16[64,32768]{1,0:T(8,128)(2,1)} reshape(bf16[2097152]{0:T(1024)(128)(2,1)} %all-gather.3.cloned.1.call-done) | data formatting | bytes 8388608 | tf_op jit(solution)/shard_map/all_gather | solution.py:17
  162.7 3.9 %fusion.29 = (bf16[64,8192]{1,0:T(8,128)(2,1)}, bf16[64,8192]{1,0:T(8,128)(2,1)}, bf16[64,8192]{1,0:T(8,128)(2,1)S(1)}, bf16[64,8192]{1,0:T(8,128)(2,1)}) fusion(bf16[64,32768]{1,0:T(8,128)(2,1)} %reshape.119), kind=kLoop, calls=%fused_computation.56 | loop fusion | bytes 8388608 | tf_op jit(solution)/shard_map/slice | solution.py:19
  166.6 2.3 reshape.114
  168.9 1.2 fusion.31
  170.1 3.3 %reshape.115 = bf16[64,2,64,64]{3,2,1,0:T(8,128)(2,1)S(1)} reshape(bf16[64,8192]{1,0:T(8,128)(2,1)} %get-tuple-element.6) | data formatting | bytes 2097152 | tf_op jit(solution)/shard_map/reshape | solution.py:19
  173.4 1.1 fusion.30
  175.6 0.9 fusion.18
  176.5 0.9 fusion.17
  177.5 2.1 collective-permute-start
  179.6 3.3 %reshape.113 = bf16[64,2,64,64]{3,2,1,0:T(8,128)(2,1)S(1)} reshape(bf16[64,8192]{1,0:T(8,128)(2,1)} %get-tuple-element.8) | data formatting | bytes 2097152 | tf_op jit(solution)/shard_map/reshape | solution.py:19
  182.9 1.2 fusion.32
  184.9 0.9 fusion.21
  186.6 6.8 %all-to-all-start = ((bf16[16,256,64]{1,2,0:T(8,128)(2,1)}), bf16[16,256,64]{1,2,0:T(8,128)(2,1)S(1)}, u32[]{:S(2)}, u32[]{:S(2)}) async-start(bf16[16,256,64]{1,2,0:T(8,128)(2,1)} %broadcast_in_dim.6), calls=%async_computation | async-start | bytes 1048576 | tf_op jit(solution)/shard_map/all_to_all | solution.py:27
  194.6 12.1 %all-to-all-done = bf16[16,256,64]{1,2,0:T(8,128)(2,1)S(1)} async-done(((bf16[16,256,64]{1,2,0:T(8,128)(2,1)}), bf16[16,256,64]{1,2,0:T(8,128)(2,1)S(1)}, u32[]{:S(2)}, u32[]{:S(2)}) %all-to-all-start) | async-done | bytes 524320 | tf_op jit(solution)/shard_map/all_to_all | solution.py:27
  206.7 1.2 fusion.6
  208.1 1.5 broadcast_in_dim.7
  209.6 3.7 %all-to-all-start.1 = ((bf16[16,256,256]{1,2,0:T(8,128)(2,1)}), bf16[16,256,256]{1,2,0:T(8,128)(2,1)S(1)}, u32[]{:S(2)}, u32[]{:S(2)}) async-start(bf16[16,256,256]{1,2,0:T(8,128)(2,1)} %broadcast_in_dim.7), calls=%async_computation.1 | async-start | bytes 4194304 | tf_op jit(solution)/shard_map/all_to_all | solution.py:27
  213.4 33.8 %all-to-all-done.1 = bf16[16,256,256]{1,2,0:T(8,128)(2,1)S(1)} async-done(((bf16[16,256,256]{1,2,0:T(8,128)(2,1)}), bf16[16,256,256]{1,2,0:T(8,128)(2,1)S(1)}, u32[]{:S(2)}, u32[]{:S(2)}) %all-to-all-start.1) | async-done | bytes 2097184 | tf_op jit(solution)/shard_map/all_to_all | solution.py:27
  250.3 1.9 collective-permute-start.1
  252.2 3.1 %collective-permute-done.1 = bf16[2,64]{0,1:T(8,128)(2,1)S(1)} collective-permute-done((bf16[2,64]{0,1:T(8,128)(2,1)S(1)}, bf16[2,64]{0,1:T(8,128)(2,1)S(1)}, u32[]{:S(2)}, u32[]{:S(2)}) %collective-permute-start.1) | collective-permute-done | bytes 288 | tf_op jit(solution)/shard_map/ppermute | solution.py:39
  256.1 13.6 %all_to_all.15 = bf16[16,256,64]{1,2,0:T(8,128)(2,1)S(1)} all-to-all(bf16[16,256,64]{1,2,0:T(8,128)(2,1)S(1)} %broadcast_in_dim.8), channel_id=1, replica_groups=mesh['sp'=64,'tp'=16] {'tp'}, dimensions={0} | all-to-all | bytes 1048576 | tf_op jit(solution)/shard_map/all_to_all | solution.py:27
  269.7 1.0 fusion.7
  (45 shorter events, 11.9 us)
Async XLA Ops:
  6.5 6.1 %copy-start.8 = (f32[2,3,64]{2,0,1:T(2,128)S(1)}, f32[2,3,64]{2,0,1:T(2,128)}, u32[]{:S(2)}) copy-start(f32[2,3,64]{2,0,1:T(2,128)} %param.13) | copy-start | bytes 4612
  6.5 6.1 %copy-start.7 = (f32[2,4096]{1,0:T(2,128)S(1)}, f32[2,4096]{1,0:T(2,128)}, u32[]{:S(2)}) copy-start(f32[2,4096]{1,0:T(2,128)} %param.8) | copy-start | bytes 98308
  6.5 148.9 %all-gather.3.cloned.1.call-start = ((), (), s32[]{:S(2)}) async-start(), calls=%async_computation.3 | async-start | bytes 4259840 | tf_op jit(solution)/shard_map/all_gather | solution.py:17
  173.4 2.0 copy-start.3
  173.4 2.2 copy-start.5
  177.5 6.6 %collective-permute-start = (bf16[2,64]{0,1:T(8,128)(2,1)S(1)}, bf16[2,64]{0,1:T(8,128)(2,1)S(1)}, u32[]{:S(2)}, u32[]{:S(2)}) collective-permute-start(bf16[2,64]{0,1:T(8,128)(2,1)S(1)} %slice.126), channel_id=1, source_target_pairs={{0,16},{16,32},{32,48},{48,64},{64,80},{80,96},{96,112},{112,128},... | collective-permute-start | bytes 776 | tf_op jit(solution)/shard_map/ppermute | solution.py:39
  182.9 2.0 copy-start.4
  184.9 8.6 %copy-start.2 = (bf16[64,8192]{1,0:T(8,128)(2,1)S(1)}, bf16[64,8192]{1,0:T(8,128)(2,1)}, u32[]{:S(2)}) copy-start(bf16[64,8192]{1,0:T(8,128)(2,1)} %get-tuple-element.5) | copy-start | bytes 3145732
  186.6 20.1 %all-to-all-start = ((bf16[16,256,64]{1,2,0:T(8,128)(2,1)}), bf16[16,256,64]{1,2,0:T(8,128)(2,1)S(1)}, u32[]{:S(2)}, u32[]{:S(2)}) async-start(bf16[16,256,64]{1,2,0:T(8,128)(2,1)} %broadcast_in_dim.6), calls=%async_computation | async-start | bytes 1048576 | tf_op jit(solution)/shard_map/all_to_all | solution.py:27
  209.6 37.5 %all-to-all-start.1 = ((bf16[16,256,256]{1,2,0:T(8,128)(2,1)}), bf16[16,256,256]{1,2,0:T(8,128)(2,1)S(1)}, u32[]{:S(2)}, u32[]{:S(2)}) async-start(bf16[16,256,256]{1,2,0:T(8,128)(2,1)} %broadcast_in_dim.7), calls=%async_computation.1 | async-start | bytes 4194304 | tf_op jit(solution)/shard_map/all_to_all | solution.py:27
  248.4 1.2 copy-start
  249.0 6.4 %copy-start.1 = (bf16[1,64,64,64]{3,2,0,1:T(8,128)(2,1)S(1)}, bf16[1,64,64,64]{3,2,0,1:T(8,128)(2,1)}, u32[]{:S(2)}) copy-start(bf16[1,64,64,64]{3,2,0,1:T(8,128)(2,1)} %get-tuple-element.13) | copy-start | bytes 1572868
  250.3 5.0 %collective-permute-start.1 = (bf16[2,64]{0,1:T(8,128)(2,1)S(1)}, bf16[2,64]{0,1:T(8,128)(2,1)S(1)}, u32[]{:S(2)}, u32[]{:S(2)}) collective-permute-start(bf16[2,64]{0,1:T(8,128)(2,1)S(1)} %slice.135), channel_id=1, source_target_pairs={{0,16},{16,32},{32,48},{48,64},{64,80},{80,96},{96,112},{112,128},... | collective-permute-start | bytes 776 | tf_op jit(solution)/shard_map/ppermute | solution.py:39
  255.4 14.3 %copy-start.6 = (bf16[1,64,16,256]{3,2,0,1:T(8,128)(2,1)S(1)}, bf16[1,64,16,256]{3,2,0,1:T(8,128)(2,1)}, u32[]{:S(2)}) copy-start(bf16[1,64,16,256]{3,2,0,1:T(8,128)(2,1)} %get-tuple-element.15) | copy-start | bytes 1572868
Sparse Core Ops, SparseCore 0:
  10.6 144.7 all-gather.2
where the time goes:
time: 278 us
  waiting for transfers between devices  192 us (69%)
  local copies, waits for them, and re-layouts  33.2 us (12%)
  starting transfers between devices  14.6 us (5%)
  between operations  13.7 us (5%)
  blocking collectives  13.6 us (5%)
  matrix products  6.57 us (2%)
  other arithmetic  4.19 us (2%)
    all_gather x1, waiting for transfers between devices, gather_packed(): lines, at, finished = (lax.all_gather(ravelled, axis), 0, [])  143 us
    all_to_all x2, waiting for transfers between devices, copy_for_each(): lax.all_to_all(jnp.broadcast_to(array[None], (length, *array.shape)), axi...  45.8 us
    all_to_all x1, blocking collectives, copy_for_each(): lax.all_to_all(jnp.broadcast_to(array[None], (length, *array.shape)), axi...  13.6 us
    all_to_all x2, starting transfers between devices, copy_for_each(): lax.all_to_all(jnp.broadcast_to(array[None], (length, *array.shape)), axi...  10.6 us
    reshape x3, local copies, waits for them, and re-layouts, gather_packed(): parts = lines[:, at:at + a.size].reshape(-1, *a.shape)  8.79 us
    all_gather x1, local copies, waits for them, and re-layouts, gather_packed(): lines, at, finished = (lax.all_gather(ravelled, axis), 0, [])  7.32 us
  transfers between devices with their start and end apart: 5, of which 4 were waited for; matrix products, arithmetic and copies ran while one was open for 3% of the time, Pallas kernels for 0%

commit v1 on v0

v1 whole, which is shorter than its diff:
```python
import functools

import jax
import jax.numpy as jnp
from jax import lax
from jax.experimental import pallas as pl
from jax.experimental.pallas import tpu as pltpu
from jax.sharding import PartitionSpec as P

EPS = 1e-06
HALO = 8
ROWS = 64
CLASS = (-4, 0, -12, 12, 4, 8, -8, 16)
OFFSETS = (
    CLASS
    + tuple(o - 1 for o in CLASS)
    + tuple(o + 1 for o in CLASS)
    + tuple(o - 2 for o in CLASS[:4])
    + tuple(o + 2 for o in CLASS[1:5])
)
VMEM = pl.BlockSpec(memory_space=pltpu.VMEM)
SMEM = pl.BlockSpec(memory_space=pltpu.SMEM)
BF16 = jnp.bfloat16
F32 = jnp.float32


def pack_kernel(wo, wi, wv, wb, *outs):
    for layer, out in enumerate(outs):
        back = wb[layer].astype(F32)
        columns = back.shape[1] // 4
        folded = jnp.concatenate(
            [back[:, k * columns : (k + 1) * columns] for k in range(4)], axis=0
        )
        parts = [w[layer].astype(F32) for w in (wo, wi, wv)] + [folded]
        out[...] = jnp.concatenate(parts, axis=1).astype(BF16)


def pack(wo, wi, wv, wb):
    shape = jax.ShapeDtypeStruct((ROWS, 4 * wo.shape[2]), BF16)
    return pl.pallas_call(
        pack_kernel,
        out_shape=[shape] * wo.shape[0],
        in_specs=[VMEM] * 4,
        out_specs=[VMEM] * wo.shape[0],
    )(wo, wi, wv, wb)


def assemble(pos, mine, other, w):
    z, core = pos[0], pos[1]
    for p, off in enumerate(OFFSETS):
        plane = lax.rem(z + (off + 32), 32)
        own = pl.multiple_of(plane * 128 + core * 64, 64)
        far = pl.multiple_of(plane * 128 + (1 - core) * 64, 64)
        w[pl.ds(own, ROWS), :] = mine[p * ROWS : (p + 1) * ROWS, :]
        w[pl.ds(far, ROWS), :] = other[p * ROWS : (p + 1) * ROWS, :]


def back_weights(w, wb):
    whole = w[:, 128:].reshape(64, 4, 16, 128)
    for k in range(4):
        wb[:, k * 128 : (k + 1) * 128] = whole[:, k].reshape(1024, 128)


def rounded(v):
    return v.astype(BF16).astype(F32)


def gate(acc, taps):
    outer, inner, value = (rounded(acc[:, k * 64 : (k + 1) * 64]) for k in range(3))
    mixed = rounded(inner * value)
    rows = mixed.shape[0]
    padded = jnp.concatenate([jnp.zeros((8, 64), F32), mixed], axis=0)
    conv = (
        taps[0:1, :] * padded[6 : 6 + rows]
        + taps[1:2, :] * padded[7 : 7 + rows]
        + taps[2:3, :] * padded[8 : 8 + rows]
    )
    return outer * conv


def store_gated(gated, out, halo):
    half = (gated.shape[0] - HALO) // 2
    main = jnp.concatenate(
        [gated[HALO : HALO + half], gated[HALO + half :]], axis=1
    ).astype(BF16)
    copies = out.shape[0]
    if halo:
        extra = jnp.concatenate([gated[:HALO], gated[:HALO]], axis=1).astype(BF16)
    for j in range(copies):
        out[j, :half, :] = main
        if halo:
            out[j, half:, :] = extra


def first_kernel(pos, x, before, gain, taps, mine, other, out, wb, w):
    assemble(pos, mine, other, w)
    back_weights(w, wb)
    chunks, width = 16, x.shape[1] // 16
    def part(k):
        cols = slice(k * width, (k + 1) * width)
        return jnp.concatenate(
            [before[:, cols].astype(F32), x[:, cols].astype(F32)], axis=0
        )
    squares = None
    for k in range(chunks):
        p = part(k)
        s = jnp.sum(p * p, axis=1, keepdims=True)
        squares = s if squares is None else squares + s
    scale = lax.rsqrt(squares / x.shape[1] + EPS)
    acc = None
    for k in range(chunks):
        cols = slice(k * width, (k + 1) * width)
        normed = (part(k) * scale * gain[0:1, cols]).astype(BF16)
        d = jnp.dot(normed, w[cols, :], preferred_element_type=F32)
        acc = d if acc is None else acc + d
    store_gated(gate(acc, taps[0]), out, True)


def second_kernel(pos, x, gain, taps, mine, other, out, wb, w):
    assemble(pos, mine, other, w)
    back_weights(w, wb)
    chunks, width = x.shape[0], x.shape[2]
    squares = None
    for k in range(chunks):
        p = x[k].astype(F32)
        s = jnp.sum(p * p, axis=1, keepdims=True)
        squares = s if squares is None else squares + s
    scale = lax.rsqrt(squares / (chunks * width) + EPS)
    acc = None
    for k in range(chunks):
        cols = slice(k * width, (k + 1) * width)
        normed = (x[k].astype(F32) * scale * gain[1:2, cols]).astype(BF16)
        d = jnp.dot(normed, w[cols, :], preferred_element_type=F32)
        acc = d if acc is None else acc + d
    store_gated(gate(acc, taps[1]), out, False)


def back_kernel(halo, gathered, wb, resid, *outs):
    count = gathered.shape[0]
    half = 128
    lefts = []
    for p in range(count // 2):
        a = gathered[2 * p].astype(F32)
        b = gathered[2 * p + 1].astype(F32)
        rows = [
            jnp.concatenate([a[:half, :64], b[:half, :64]], axis=1),
            jnp.concatenate([a[:half, 64:], b[:half, 64:]], axis=1),
        ]
        if halo:
            rows = [jnp.concatenate([a[half:, :64], b[half:, :64]], axis=1)] + rows
        lefts.append(jnp.concatenate(rows, axis=0).astype(BF16))
    left = jnp.concatenate(lefts, axis=1)
    wide = jnp.dot(left, wb[...], preferred_element_type=F32)
    proj = jnp.concatenate(
        [wide[:, k * 128 + 64 : (k + 1) * 128] for k in range(4)], axis=1
    )
    start = resid.shape[0] - proj.shape[0]
    new = (resid[...].astype(F32)[start:] + proj).astype(BF16)
    if halo:
        outs[0][...] = new
        for j in range(count):
            outs[1][j, :, :] = new
    else:
        outs[0][...] = new


def call(kernel, out_shape, n_in, smem=False, scratch=(), flops=0, moved=0):
    specs = ([SMEM] if smem else []) + [VMEM] * (n_in - int(smem))
    return pl.pallas_call(
        kernel,
        out_shape=out_shape,
        in_specs=specs,
        out_specs=jax.tree.map(lambda _: VMEM, out_shape),
        scratch_shapes=scratch,
        cost_estimate=pl.CostEstimate(flops=flops, bytes_accessed=moved, transcendentals=0),
    )


def exchange(block, distance):
    return lax.ppermute(
        block, "sp", [(i, (i + 2 * distance) % 64) for i in range(64)]
    )


def gather_planes(block):
    low = exchange(block, 12)
    high = exchange(block, -12)
    half = ROWS // 2
    up = exchange(jnp.concatenate([block, high, low[:half]], axis=0), 4)
    down = exchange(jnp.concatenate([block, low, high[half:]], axis=0), -4)
    first, second = slice(0, ROWS), slice(ROWS, 2 * ROWS)
    own = jnp.concatenate(
        [up[first], block, low, high, down[first], up[second], down[second]]
        + [up[2 * ROWS :], down[2 * ROWS :]],
        axis=0,
    )
    a = exchange(own, 1)
    b = exchange(own, -1)
    c = exchange(own[: 4 * ROWS], 2)
    d = exchange(own[ROWS : 5 * ROWS], -2)
    mine = jnp.concatenate([own, a, b, c, d], axis=0)
    other = lax.ppermute(mine, "sp", [(i, i ^ 1) for i in range(64)])
    return mine, other


def per_device(tokens, norm_gain, w_outer, w_inner, w_value, w_back, taps):
    count, width = tokens.shape
    feats = w_back.shape[2]
    own = lax.axis_index("tp")
    sp = lax.axis_index("sp")
    pos = jnp.stack([sp // 2, sp % 2]).astype(jnp.int32)
    tp = lax.axis_size("tp")

    packed = pack(w_outer, w_inner, w_value, w_back)
    before = lax.ppermute(tokens[count - HALO :], "sp", [(i, i + 1) for i in range(63)])
    held = [gather_planes(block) for block in packed]

    rows = count + HALO
    resid = lax.dynamic_slice_in_dim(
        jnp.concatenate([before, tokens], axis=0), own * feats, feats, 1
    )
    weights = pltpu.VMEM((width, 256), BF16)
    back_shape = jax.ShapeDtypeStruct((1024, 512), BF16)
    flops = 2 * rows * width * 256
    swap = functools.partial(
        lax.all_to_all, axis_name="tp", split_axis=0, concat_axis=0, tiled=True
    )

    gated, back = call(
        first_kernel,
        [jax.ShapeDtypeStruct((tp, count // 2 + HALO, 128), BF16), back_shape],
        7, True, [weights], flops, 8 << 20,
    )(pos, tokens, before, norm_gain, taps, *held[0])
    whole = swap(gated)
    resid, spread = call(
        functools.partial(back_kernel, True),
        [
            jax.ShapeDtypeStruct((rows, feats), BF16),
            jax.ShapeDtypeStruct((tp, rows, feats), BF16),
        ],
        3, False, [], 2 * rows * 1024 * 512, 4 << 20,
    )(whole, back, resid)
    current = swap(spread)
    gated, back = call(
        second_kernel,
        [jax.ShapeDtypeStruct((tp, count // 2, 128), BF16), back_shape],
        6, True, [weights], flops, 8 << 20,
    )(pos, current, norm_gain, taps, *held[1])
    whole = swap(gated)
    (result,) = call(
        functools.partial(back_kernel, False),
        [jax.ShapeDtypeStruct((count, feats), BF16)],
        3, False, [], 2 * rows * 1024 * 512, 4 << 20,
    )(whole, back, resid)
    return result


def solution(mesh):
    in_specs = (
        P("sp", None),
        P(),
        P(None, "sp", "tp"),
        P(None, "sp", "tp"),
        P(None, "sp", "tp"),
        P(None, "sp", "tp"),
        P(None, None, "tp"),
    )
    out_specs = P("sp", "tp")
    return jax.shard_map(
        per_device, mesh=mesh, in_specs=in_specs, out_specs=out_specs, check_vma=False
    )
```

time: 278 us -> 233 us (0.84)
  the two profiles are of different devices: /device:TPU:32 before, /device:TPU:1 now
where the time goes in v1:
time: 233 us; the launch traced here: 232 us
  starting transfers between devices  126 us (54%)
  waiting for transfers between devices  52.5 us (23%)
  Pallas kernels  17.9 us (8%)
  blocking collectives  17.7 us (8%)
  local copies, waits for them, and re-layouts  14.7 us (6%)
  other arithmetic  2.93 us (1%)
    ppermute x16, starting transfers between devices, exchange(): lax.ppermute(block, 'sp', [(i, (i + 2 * distance) % 64) for i in range(64)])  92.6 us
    ppermute x16, waiting for transfers between devices, exchange(): lax.ppermute(block, 'sp', [(i, (i + 2 * distance) % 64) for i in range(64)])  42.8 us
    ppermute x2, starting transfers between devices, gather_planes(): other = lax.ppermute(mine, 'sp', [(i, i ^ 1) for i in range(64)])  18.4 us
    all_to_all x1, blocking collectives, per_device(): whole = swap(gated)  17.7 us
    unnamed x37, local copies, waits for them, and re-layouts  11.5 us
    all_to_all x1, waiting for transfers between devices, per_device(): whole = swap(gated)  7.05 us
    all_to_all x1, starting transfers between devices, per_device(): whole = swap(gated)  6.28 us
    pallas_call x1, Pallas kernels, per_device(): call(first_kernel, [jax.ShapeDtypeStruct((tp, count // 2 + HALO, 128), BF...  5.08 us
  transfers between devices with their start and end apart: 21, of which 9 were waited for; matrix products, arithmetic and copies ran while one was open for 6% of the time, Pallas kernels for 2%

profile of v1, /device:TPU:1, one launch (start us, length us, event | category | flops | bytes accessed | tf_op | source)
XLA Modules:
  0.0 231.9 jit_solution(8558498311563877564)
XLA Ops:
  1.7 23.0 %collective-permute-start.2 = (bf16[64,256]{1,0:T(8,128)(2,1)}, bf16[64,256]{1,0:T(8,128)(2,1)S(1)}, u32[]{:S(2)}, u32[]{:S(2)}) collective-permute-start(bf16[64,256]{1,0:T(8,128)(2,1)} %get-tuple-element.13), channel_id=1, source_target_pairs={{0,384},{16,400},{32,416},{48,432},{64,448},{80,464},{96,480},{112... | collective-permute-start | bytes 98312 | tf_op jit(solution)/shard_map/ppermute | solution.py:180
  24.7 5.6 %collective-permute-start.1 = (bf16[64,256]{1,0:T(8,128)(2,1)}, bf16[64,256]{1,0:T(8,128)(2,1)S(1)}, u32[]{:S(2)}, u32[]{:S(2)}) collective-permute-start(bf16[64,256]{1,0:T(8,128)(2,1)} %get-tuple-element.13), channel_id=1, source_target_pairs={{0,640},{16,656},{32,672},{48,688},{64,704},{80,720},{96,736},{112... | collective-permute-start | bytes 98312 | tf_op jit(solution)/shard_map/ppermute | solution.py:180
  30.3 12.8 %collective-permute-done.1 = bf16[64,256]{1,0:T(8,128)(2,1)S(1)} collective-permute-done((bf16[64,256]{1,0:T(8,128)(2,1)}, bf16[64,256]{1,0:T(8,128)(2,1)S(1)}, u32[]{:S(2)}, u32[]{:S(2)}) %collective-permute-start.1) | collective-permute-done | bytes 32800 | tf_op jit(solution)/shard_map/ppermute | solution.py:180
  43.9 8.8 %collective-permute-start.3 = (bf16[160,256]{1,0:T(8,128)(2,1)S(1)}, bf16[160,256]{1,0:T(8,128)(2,1)S(1)}, u32[]{:S(2)}, u32[]{:S(2)}) collective-permute-start(bf16[160,256]{1,0:T(8,128)(2,1)S(1)} %get-tuple-element.68), channel_id=1, source_target_pairs={{0,128},{16,144},{32,160},{48,176},{64,192},{80,208},{96,224},{112... | collective-permute-start | bytes 245768 | tf_op jit(solution)/shard_map/ppermute | solution.py:180
  56.1 7.4 %collective-permute-done.4 = bf16[160,256]{1,0:T(8,128)(2,1)S(1)} collective-permute-done((bf16[160,256]{1,0:T(8,128)(2,1)S(1)}, bf16[160,256]{1,0:T(8,128)(2,1)S(1)}, u32[]{:S(2)}, u32[]{:S(2)}) %collective-permute-start.4) | collective-permute-done | bytes 81952 | tf_op jit(solution)/shard_map/ppermute | solution.py:180
  66.3 3.8 %collective-permute-start.6 = (bf16[512,256]{1,0:T(8,128)(2,1)S(1)}, bf16[512,256]{1,0:T(8,128)(2,1)S(1)}, u32[]{:S(2)}, u32[]{:S(2)}) collective-permute-start(bf16[512,256]{1,0:T(8,128)(2,1)S(1)} %get-tuple-element.45), channel_id=1, source_target_pairs={{0,992},{16,1008},{32,0},{48,16},{64,32},{80,48},{96,64},{112,80},... | collective-permute-start | bytes 786440 | tf_op jit(solution)/shard_map/ppermute | solution.py:180
  72.9 4.3 %collective-permute-start.7 = (bf16[256,256]{1,0:T(8,128)(2,1)S(1)}, bf16[256,256]{1,0:T(8,128)(2,1)S(1)}, u32[]{:S(2)}, u32[]{:S(2)}) collective-permute-start(bf16[256,256]{1,0:T(8,128)(2,1)S(1)} %get-tuple-element.24), channel_id=1, source_target_pairs={{0,64},{16,80},{32,96},{48,112},{64,128},{80,144},{96,160},{112,17... | collective-permute-start | bytes 393224 | tf_op jit(solution)/shard_map/ppermute | solution.py:180
  77.2 4.5 %collective-permute-done.7 = bf16[256,256]{1,0:T(8,128)(2,1)S(1)} collective-permute-done((bf16[256,256]{1,0:T(8,128)(2,1)S(1)}, bf16[256,256]{1,0:T(8,128)(2,1)S(1)}, u32[]{:S(2)}, u32[]{:S(2)}) %collective-permute-start.7) | collective-permute-done | bytes 131104 | tf_op jit(solution)/shard_map/ppermute | solution.py:180
  81.7 10.8 %collective-permute-start.9 = (bf16[2048,256]{1,0:T(8,128)(2,1)S(1)}, bf16[2048,256]{1,0:T(8,128)(2,1)}, u32[]{:S(2)}, u32[]{:S(2)}) collective-permute-start(bf16[2048,256]{1,0:T(8,128)(2,1)S(1)} %constant_dynamic-update-slice_fusion.9.mine), channel_id=1, source_target_pairs={{0,16},{16,0},{32,48},{48,32},{64,80},{80,64},{96,112},{112,96},{1... | collective-permute-start | bytes 3145736 | tf_op jit(solution)/shard_map/ppermute | solution.py:202
  92.5 9.0 %collective-permute-start.11 = (bf16[64,256]{1,0:T(8,128)(2,1)S(1)}, bf16[64,256]{1,0:T(8,128)(2,1)S(1)}, u32[]{:S(2)}, u32[]{:S(2)}) collective-permute-start(bf16[64,256]{1,0:T(8,128)(2,1)S(1)} %copy-done.4), channel_id=1, source_target_pairs={{0,384},{16,400},{32,416},{48,432},{64,448},{80,464},{96,480},{112... | collective-permute-start | bytes 98312 | tf_op jit(solution)/shard_map/ppermute | solution.py:180
  101.5 9.8 %collective-permute-start.10 = (bf16[64,256]{1,0:T(8,128)(2,1)S(1)}, bf16[64,256]{1,0:T(8,128)(2,1)S(1)}, u32[]{:S(2)}, u32[]{:S(2)}) collective-permute-start(bf16[64,256]{1,0:T(8,128)(2,1)S(1)} %copy-done.4), channel_id=1, source_target_pairs={{0,640},{16,656},{32,672},{48,688},{64,704},{80,720},{96,736},{112... | collective-permute-start | bytes 98312 | tf_op jit(solution)/shard_map/ppermute | solution.py:180
  112.0 4.8 %collective-permute-start = (bf16[8,4096]{1,0:T(8,128)(2,1)}, bf16[8,4096]{1,0:T(8,128)(2,1)S(1)}, u32[]{:S(2)}, u32[]{:S(2)}) collective-permute-start(bf16[8,4096]{1,0:T(8,128)(2,1)} %slice.59), channel_id=1, source_target_pairs={{0,16},{16,32},{32,48},{48,64},{64,80},{80,96},{96,112},{112,128},... | collective-permute-start | bytes 196616 | tf_op jit(solution)/shard_map/ppermute | solution.py:215
  118.1 5.0 %collective-permute-done.10 = bf16[64,256]{1,0:T(8,128)(2,1)S(1)} collective-permute-done((bf16[64,256]{1,0:T(8,128)(2,1)S(1)}, bf16[64,256]{1,0:T(8,128)(2,1)S(1)}, u32[]{:S(2)}, u32[]{:S(2)}) %collective-permute-start.10) | collective-permute-done | bytes 32800 | tf_op jit(solution)/shard_map/ppermute | solution.py:180
  123.1 5.2 %collective-permute-start.13 = (bf16[160,256]{1,0:T(8,128)(2,1)S(1)}, bf16[160,256]{1,0:T(8,128)(2,1)S(1)}, u32[]{:S(2)}, u32[]{:S(2)}) collective-permute-start(bf16[160,256]{1,0:T(8,128)(2,1)S(1)} %get-tuple-element.59), channel_id=1, source_target_pairs={{0,896},{16,912},{32,928},{48,944},{64,960},{80,976},{96,992},{112... | collective-permute-start | bytes 245768 | tf_op jit(solution)/shard_map/ppermute | solution.py:180
  128.3 4.0 %collective-permute-start.12 = (bf16[160,256]{1,0:T(8,128)(2,1)S(1)}, bf16[160,256]{1,0:T(8,128)(2,1)S(1)}, u32[]{:S(2)}, u32[]{:S(2)}) collective-permute-start(bf16[160,256]{1,0:T(8,128)(2,1)S(1)} %get-tuple-element.60), channel_id=1, source_target_pairs={{0,128},{16,144},{32,160},{48,176},{64,192},{80,208},{96,224},{112... | collective-permute-start | bytes 245768 | tf_op jit(solution)/shard_map/ppermute | solution.py:180
  133.0 6.8 %collective-permute-done.12 = bf16[160,256]{1,0:T(8,128)(2,1)S(1)} collective-permute-done((bf16[160,256]{1,0:T(8,128)(2,1)S(1)}, bf16[160,256]{1,0:T(8,128)(2,1)S(1)}, u32[]{:S(2)}, u32[]{:S(2)}) %collective-permute-start.12) | collective-permute-done | bytes 81952 | tf_op jit(solution)/shard_map/ppermute | solution.py:180
  142.9 5.1 %shard_map.74 = (bf16[16,136,128]{2,1,0:T(8,128)(2,1)}, bf16[1024,512]{1,0:T(8,128)(2,1)}) custom-call(s32[2]{0:T(128)} %pad_add_fusion.pos, bf16[256,4096]{1,0:T(8,128)(2,1)} %x.1, bf16[8,4096]{1,0:T(8,128)(2,1)} %copy-done.5, f32[2,4096]{1,0:T(2,128)} %gain.3, f32[2,3,64]{2,1,0:T(4,128)} %copy.8.taps, bf16[2048,256]{1,0:T(8,128)(2,1)} %copy-done.3, ...), custom_call_target="tpu_custom_call" | custom-call | flops 553648128 | bytes 8388608 | tf_op jit(solution)/shard_map/pallas_call | solution.py:229
  147.9 6.3 %all-to-all-start = ((bf16[16,136,128]{2,1,0:T(8,128)(2,1)}), bf16[16,136,128]{2,1,0:T(8,128)(2,1)S(1)}, u32[]{:S(2)}, u32[]{:S(2)}) async-start(bf16[16,136,128]{2,1,0:T(8,128)(2,1)} %get-tuple-element.14), calls=%async_computation | async-start | bytes 1114112 | tf_op jit(solution)/shard_map/all_to_all | solution.py:234
  156.8 7.0 %all-to-all-done.gathered = bf16[16,136,128]{2,1,0:T(8,128)(2,1)S(1)} async-done(((bf16[16,136,128]{2,1,0:T(8,128)(2,1)}), bf16[16,136,128]{2,1,0:T(8,128)(2,1)S(1)}, u32[]{:S(2)}, u32[]{:S(2)}) %all-to-all-start) | async-done | bytes 557088 | tf_op jit(solution)/shard_map/all_to_all | solution.py:234
  175.7 4.6 %collective-permute-start.15 = (bf16[512,256]{1,0:T(8,128)(2,1)}, bf16[512,256]{1,0:T(8,128)(2,1)S(1)}, u32[]{:S(2)}, u32[]{:S(2)}) collective-permute-start(bf16[512,256]{1,0:T(8,128)(2,1)} %get-tuple-element.31), channel_id=1, source_target_pairs={{0,992},{16,1008},{32,0},{48,16},{64,32},{80,48},{96,64},{112,80},... | collective-permute-start | bytes 786440 | tf_op jit(solution)/shard_map/ppermute | solution.py:180
  188.0 5.7 %collective-permute-done.16 = bf16[256,256]{1,0:T(8,128)(2,1)S(1)} collective-permute-done((bf16[256,256]{1,0:T(8,128)(2,1)S(1)}, bf16[256,256]{1,0:T(8,128)(2,1)S(1)}, u32[]{:S(2)}, u32[]{:S(2)}) %collective-permute-start.16) | collective-permute-done | bytes 131104 | tf_op jit(solution)/shard_map/ppermute | solution.py:180
  195.0 7.6 %collective-permute-start.18 = (bf16[2048,256]{1,0:T(8,128)(2,1)}, bf16[2048,256]{1,0:T(8,128)(2,1)}, u32[]{:S(2)}, u32[]{:S(2)}) collective-permute-start(bf16[2048,256]{1,0:T(8,128)(2,1)} %constant_dynamic-update-slice_fusion.31.mine), channel_id=1, source_target_pairs={{0,16},{16,0},{32,48},{48,32},{64,80},{80,64},{96,112},{112,96},{1... | collective-permute-start | bytes 3145736 | tf_op jit(solution)/shard_map/ppermute | solution.py:202
  206.6 5.1 %shard_map.76 = (bf16[16,128,128]{2,1,0:T(8,128)(2,1)}, bf16[1024,512]{1,0:T(8,128)(2,1)}) custom-call(s32[2]{0:T(128)} %pad_add_fusion.pos, bf16[16,264,256]{2,1,0:T(8,128)(2,1)} %copy-done.1, f32[2,4096]{1,0:T(2,128)} %gain.3, f32[2,3,64]{2,1,0:T(4,128)} %copy.8.taps, bf16[2048,256]{1,0:T(8,128)(2,1)} %constant_dynamic-update-slice_fusion.31.mine, ...), custom_call_target="tpu_custom_call" | custom-call | flops 553648128 | bytes 8388608 | tf_op jit(solution)/shard_map/pallas_call | solution.py:244
  211.6 17.7 %all_to_all.15.gathered = bf16[16,128,128]{2,1,0:T(8,128)(2,1)} all-to-all(bf16[16,128,128]{2,1,0:T(8,128)(2,1)} %get-tuple-element.18), channel_id=1, replica_groups=mesh['sp'=64,'tp'=16] {'tp'}, dimensions={0} | all-to-all | bytes 1048576 | tf_op jit(solution)/shard_map/all_to_all | solution.py:249
  (80 shorter events, 47.0 us)
Async XLA Ops:
  0.0 111.4 %copy-start = (bf16[256,4096]{1,0:T(8,128)(2,1)S(1)}, bf16[256,4096]{1,0:T(8,128)(2,1)}, u32[]{:S(2)}) copy-start(bf16[256,4096]{1,0:T(8,128)(2,1)} %x.1) | copy-start | bytes 6291460
  0.0 117.5 %copy-start.8 = (f32[2,3,64]{2,0,1:T(2,128)S(1)}, f32[2,3,64]{2,0,1:T(2,128)}, u32[]{:S(2)}) copy-start(f32[2,3,64]{2,0,1:T(2,128)} %param.13) | copy-start | bytes 4612
  1.7 90.8 %copy-start.4 = (bf16[64,256]{1,0:T(8,128)(2,1)S(1)}, bf16[64,256]{1,0:T(8,128)(2,1)}, u32[]{:S(2)}) copy-start(bf16[64,256]{1,0:T(8,128)(2,1)} %get-tuple-element.17) | copy-start | bytes 98308
  1.7 28.6 %collective-permute-start.2 = (bf16[64,256]{1,0:T(8,128)(2,1)}, bf16[64,256]{1,0:T(8,128)(2,1)S(1)}, u32[]{:S(2)}, u32[]{:S(2)}) collective-permute-start(bf16[64,256]{1,0:T(8,128)(2,1)} %get-tuple-element.13), channel_id=1, source_target_pairs={{0,384},{16,400},{32,416},{48,432},{64,448},{80,464},{96,480},{112... | collective-permute-start | bytes 98312 | tf_op jit(solution)/shard_map/ppermute | solution.py:180
  24.7 18.4 %collective-permute-start.1 = (bf16[64,256]{1,0:T(8,128)(2,1)}, bf16[64,256]{1,0:T(8,128)(2,1)S(1)}, u32[]{:S(2)}, u32[]{:S(2)}) collective-permute-start(bf16[64,256]{1,0:T(8,128)(2,1)} %get-tuple-element.13), channel_id=1, source_target_pairs={{0,640},{16,656},{32,672},{48,688},{64,704},{80,720},{96,736},{112... | collective-permute-start | bytes 98312 | tf_op jit(solution)/shard_map/ppermute | solution.py:180
  43.9 11.4 %collective-permute-start.3 = (bf16[160,256]{1,0:T(8,128)(2,1)S(1)}, bf16[160,256]{1,0:T(8,128)(2,1)S(1)}, u32[]{:S(2)}, u32[]{:S(2)}) collective-permute-start(bf16[160,256]{1,0:T(8,128)(2,1)S(1)} %get-tuple-element.68), channel_id=1, source_target_pairs={{0,128},{16,144},{32,160},{48,176},{64,192},{80,208},{96,224},{112... | collective-permute-start | bytes 245768 | tf_op jit(solution)/shard_map/ppermute | solution.py:180
  52.7 10.8 %collective-permute-start.4 = (bf16[160,256]{1,0:T(8,128)(2,1)S(1)}, bf16[160,256]{1,0:T(8,128)(2,1)S(1)}, u32[]{:S(2)}, u32[]{:S(2)}) collective-permute-start(bf16[160,256]{1,0:T(8,128)(2,1)S(1)} %get-tuple-element.67), channel_id=1, source_target_pairs={{0,896},{16,912},{32,928},{48,944},{64,960},{80,976},{96,992},{112... | collective-permute-start | bytes 245768 | tf_op jit(solution)/shard_map/ppermute | solution.py:180
  63.6 13.6 %collective-permute-start.5 = (bf16[512,256]{1,0:T(8,128)(2,1)S(1)}, bf16[512,256]{1,0:T(8,128)(2,1)S(1)}, u32[]{:S(2)}, u32[]{:S(2)}) collective-permute-start(bf16[512,256]{1,0:T(8,128)(2,1)S(1)} %get-tuple-element.45), channel_id=1, source_target_pairs={{0,32},{16,48},{32,64},{48,80},{64,96},{80,112},{96,128},{112,144}... | collective-permute-start | bytes 786440 | tf_op jit(solution)/shard_map/ppermute | solution.py:180
  66.3 10.9 %collective-permute-start.6 = (bf16[512,256]{1,0:T(8,128)(2,1)S(1)}, bf16[512,256]{1,0:T(8,128)(2,1)S(1)}, u32[]{:S(2)}, u32[]{:S(2)}) collective-permute-start(bf16[512,256]{1,0:T(8,128)(2,1)S(1)} %get-tuple-element.45), channel_id=1, source_target_pairs={{0,992},{16,1008},{32,0},{48,16},{64,32},{80,48},{96,64},{112,80},... | collective-permute-start | bytes 786440 | tf_op jit(solution)/shard_map/ppermute | solution.py:180
  70.9 10.8 %collective-permute-start.8 = (bf16[256,256]{1,0:T(8,128)(2,1)S(1)}, bf16[256,256]{1,0:T(8,128)(2,1)S(1)}, u32[]{:S(2)}, u32[]{:S(2)}) collective-permute-start(bf16[256,256]{1,0:T(8,128)(2,1)S(1)} %get-tuple-element.23), channel_id=1, source_target_pairs={{0,960},{16,976},{32,992},{48,1008},{64,0},{80,16},{96,32},{112,48... | collective-permute-start | bytes 393224 | tf_op jit(solution)/shard_map/ppermute | solution.py:180
  72.9 8.8 %collective-permute-start.7 = (bf16[256,256]{1,0:T(8,128)(2,1)S(1)}, bf16[256,256]{1,0:T(8,128)(2,1)S(1)}, u32[]{:S(2)}, u32[]{:S(2)}) collective-permute-start(bf16[256,256]{1,0:T(8,128)(2,1)S(1)} %get-tuple-element.24), channel_id=1, source_target_pairs={{0,64},{16,80},{32,96},{48,112},{64,128},{80,144},{96,160},{112,17... | collective-permute-start | bytes 393224 | tf_op jit(solution)/shard_map/ppermute | solution.py:180
  81.7 61.1 %collective-permute-start.9 = (bf16[2048,256]{1,0:T(8,128)(2,1)S(1)}, bf16[2048,256]{1,0:T(8,128)(2,1)}, u32[]{:S(2)}, u32[]{:S(2)}) collective-permute-start(bf16[2048,256]{1,0:T(8,128)(2,1)S(1)} %constant_dynamic-update-slice_fusion.9.mine), channel_id=1, source_target_pairs={{0,16},{16,0},{32,48},{48,32},{64,80},{80,64},{96,112},{112,96},{1... | collective-permute-start | bytes 3145736 | tf_op jit(solution)/shard_map/ppermute | solution.py:202
  92.5 25.5 %collective-permute-start.11 = (bf16[64,256]{1,0:T(8,128)(2,1)S(1)}, bf16[64,256]{1,0:T(8,128)(2,1)S(1)}, u32[]{:S(2)}, u32[]{:S(2)}) collective-permute-start(bf16[64,256]{1,0:T(8,128)(2,1)S(1)} %copy-done.4), channel_id=1, source_target_pairs={{0,384},{16,400},{32,416},{48,432},{64,448},{80,464},{96,480},{112... | collective-permute-start | bytes 98312 | tf_op jit(solution)/shard_map/ppermute | solution.py:180
  101.5 21.6 %collective-permute-start.10 = (bf16[64,256]{1,0:T(8,128)(2,1)S(1)}, bf16[64,256]{1,0:T(8,128)(2,1)S(1)}, u32[]{:S(2)}, u32[]{:S(2)}) collective-permute-start(bf16[64,256]{1,0:T(8,128)(2,1)S(1)} %copy-done.4), channel_id=1, source_target_pairs={{0,640},{16,656},{32,672},{48,688},{64,704},{80,720},{96,736},{112... | collective-permute-start | bytes 98312 | tf_op jit(solution)/shard_map/ppermute | solution.py:180
  112.0 20.3 %collective-permute-start = (bf16[8,4096]{1,0:T(8,128)(2,1)}, bf16[8,4096]{1,0:T(8,128)(2,1)S(1)}, u32[]{:S(2)}, u32[]{:S(2)}) collective-permute-start(bf16[8,4096]{1,0:T(8,128)(2,1)} %slice.59), channel_id=1, source_target_pairs={{0,16},{16,32},{32,48},{48,64},{64,80},{80,96},{96,112},{112,128},... | collective-permute-start | bytes 196616 | tf_op jit(solution)/shard_map/ppermute | solution.py:215
  123.1 31.1 %collective-permute-start.13 = (bf16[160,256]{1,0:T(8,128)(2,1)S(1)}, bf16[160,256]{1,0:T(8,128)(2,1)S(1)}, u32[]{:S(2)}, u32[]{:S(2)}) collective-permute-start(bf16[160,256]{1,0:T(8,128)(2,1)S(1)} %get-tuple-element.59), channel_id=1, source_target_pairs={{0,896},{16,912},{32,928},{48,944},{64,960},{80,976},{96,992},{112... | collective-permute-start | bytes 245768 | tf_op jit(solution)/shard_map/ppermute | solution.py:180
  128.3 11.5 %collective-permute-start.12 = (bf16[160,256]{1,0:T(8,128)(2,1)S(1)}, bf16[160,256]{1,0:T(8,128)(2,1)S(1)}, u32[]{:S(2)}, u32[]{:S(2)}) collective-permute-start(bf16[160,256]{1,0:T(8,128)(2,1)S(1)} %get-tuple-element.60), channel_id=1, source_target_pairs={{0,128},{16,144},{32,160},{48,176},{64,192},{80,208},{96,224},{112... | collective-permute-start | bytes 245768 | tf_op jit(solution)/shard_map/ppermute | solution.py:180
  147.9 15.9 %all-to-all-start = ((bf16[16,136,128]{2,1,0:T(8,128)(2,1)}), bf16[16,136,128]{2,1,0:T(8,128)(2,1)S(1)}, u32[]{:S(2)}, u32[]{:S(2)}) async-start(bf16[16,136,128]{2,1,0:T(8,128)(2,1)} %get-tuple-element.14), calls=%async_computation | async-start | bytes 1114112 | tf_op jit(solution)/shard_map/all_to_all | solution.py:234
  168.1 37.1 %all-to-all-start.1 = ((bf16[16,264,256]{2,1,0:T(8,128)(2,1)}), bf16[16,264,256]{2,1,0:T(8,128)(2,1)S(1)}, u32[]{:S(2)}, u32[]{:S(2)}) async-start(bf16[16,264,256]{2,1,0:T(8,128)(2,1)} %get-tuple-element.16), calls=%async_computation.1 | async-start | bytes 4325376 | tf_op jit(solution)/shard_map/all_to_all | solution.py:243
  173.8 12.7 %collective-permute-start.14 = (bf16[512,256]{1,0:T(8,128)(2,1)}, bf16[512,256]{1,0:T(8,128)(2,1)S(1)}, u32[]{:S(2)}, u32[]{:S(2)}) collective-permute-start(bf16[512,256]{1,0:T(8,128)(2,1)} %get-tuple-element.31), channel_id=1, source_target_pairs={{0,32},{16,48},{32,64},{48,80},{64,96},{80,112},{96,128},{112,144}... | collective-permute-start | bytes 786440 | tf_op jit(solution)/shard_map/ppermute | solution.py:180
  175.7 11.6 %collective-permute-start.15 = (bf16[512,256]{1,0:T(8,128)(2,1)}, bf16[512,256]{1,0:T(8,128)(2,1)S(1)}, u32[]{:S(2)}, u32[]{:S(2)}) collective-permute-start(bf16[512,256]{1,0:T(8,128)(2,1)} %get-tuple-element.31), channel_id=1, source_target_pairs={{0,992},{16,1008},{32,0},{48,16},{64,32},{80,48},{96,64},{112,80},... | collective-permute-start | bytes 786440 | tf_op jit(solution)/shard_map/ppermute | solution.py:180
  180.3 14.0 %collective-permute-start.17 = (bf16[256,256]{1,0:T(8,128)(2,1)S(1)}, bf16[256,256]{1,0:T(8,128)(2,1)S(1)}, u32[]{:S(2)}, u32[]{:S(2)}) collective-permute-start(bf16[256,256]{1,0:T(8,128)(2,1)S(1)} %get-tuple-element.21), channel_id=1, source_target_pairs={{0,960},{16,976},{32,992},{48,1008},{64,0},{80,16},{96,32},{112,48... | collective-permute-start | bytes 393224 | tf_op jit(solution)/shard_map/ppermute | solution.py:180
  182.7 11.0 %collective-permute-start.16 = (bf16[256,256]{1,0:T(8,128)(2,1)S(1)}, bf16[256,256]{1,0:T(8,128)(2,1)S(1)}, u32[]{:S(2)}, u32[]{:S(2)}) collective-permute-start(bf16[256,256]{1,0:T(8,128)(2,1)S(1)} %get-tuple-element.22), channel_id=1, source_target_pairs={{0,64},{16,80},{32,96},{48,112},{64,128},{80,144},{96,160},{112,17... | collective-permute-start | bytes 393224 | tf_op jit(solution)/shard_map/ppermute | solution.py:180
  195.0 10.2 %collective-permute-start.18 = (bf16[2048,256]{1,0:T(8,128)(2,1)}, bf16[2048,256]{1,0:T(8,128)(2,1)}, u32[]{:S(2)}, u32[]{:S(2)}) collective-permute-start(bf16[2048,256]{1,0:T(8,128)(2,1)} %constant_dynamic-update-slice_fusion.31.mine), channel_id=1, source_target_pairs={{0,16},{16,0},{32,48},{48,32},{64,80},{80,64},{96,112},{112,96},{1... | collective-permute-start | bytes 3145736 | tf_op jit(solution)/shard_map/ppermute | solution.py:202
  (6 other events, 85.8 us)

commit v2 on v1

--- a/solution.py
+++ b/solution.py
@@ -10,49 +10,35 @@
 EPS = 1e-06
 HALO = 8
 ROWS = 64
-CLASS = (-4, 0, -12, 12, 4, 8, -8, 16)
-OFFSETS = (
-    CLASS
-    + tuple(o - 1 for o in CLASS)
-    + tuple(o + 1 for o in CLASS)
-    + tuple(o - 2 for o in CLASS[:4])
-    + tuple(o + 2 for o in CLASS[1:5])
-)
 VMEM = pl.BlockSpec(memory_space=pltpu.VMEM)
-SMEM = pl.BlockSpec(memory_space=pltpu.SMEM)
 BF16 = jnp.bfloat16
 F32 = jnp.float32
 
 
-def pack_kernel(wo, wi, wv, wb, *outs):
-    for layer, out in enumerate(outs):
+def pack_kernel(wo, wi, wv, wb, out):
+    for layer in range(out.shape[0]):
         back = wb[layer].astype(F32)
         columns = back.shape[1] // 4
         folded = jnp.concatenate(
             [back[:, k * columns : (k + 1) * columns] for k in range(4)], axis=0
         )
         parts = [w[layer].astype(F32) for w in (wo, wi, wv)] + [folded]
-        out[...] = jnp.concatenate(parts, axis=1).astype(BF16)
-
-
-def pack(wo, wi, wv, wb):
-    shape = jax.ShapeDtypeStruct((ROWS, 4 * wo.shape[2]), BF16)
-    return pl.pallas_call(
-        pack_kernel,
-        out_shape=[shape] * wo.shape[0],
-        in_specs=[VMEM] * 4,
-        out_specs=[VMEM] * wo.shape[0],
-    )(wo, wi, wv, wb)
-
-
-def assemble(pos, mine, other, w):
-    z, core = pos[0], pos[1]
-    for p, off in enumerate(OFFSETS):
-        plane = lax.rem(z + (off + 32), 32)
-        own = pl.multiple_of(plane * 128 + core * 64, 64)
-        far = pl.multiple_of(plane * 128 + (1 - core) * 64, 64)
-        w[pl.ds(own, ROWS), :] = mine[p * ROWS : (p + 1) * ROWS, :]
-        w[pl.ds(far, ROWS), :] = other[p * ROWS : (p + 1) * ROWS, :]
+        out[layer] = jnp.concatenate(parts, axis=1).astype(BF16)
+
+
+def assemble(blocks, w):
+    own, own_far, near, near_far = blocks
+    sp = lax.axis_index("sp")
+    plane, core = lax.rem(lax.div(sp, 2), 4), lax.rem(sp, 2)
+    for shift, part, count in ((0, None, 8), (3, 0, 8), (1, 8, 8), (2, 16, 8)):
+        residue = lax.rem(plane + shift, 4)
+        for side, (first, rest) in enumerate(((own, near), (own_far, near_far))):
+            start = 128 * residue + 64 * (core if side == 0 else 1 - core)
+            for k in range(count):
+                source = first if part is None else rest
+                at = (k if part is None else part + k) * ROWS
+                row = pl.multiple_of(512 * k + start, 64)
+                w[pl.ds(row, ROWS), :] = source[at : at + ROWS, :]
 
 
 def back_weights(w, wb):
@@ -92,8 +78,8 @@
             out[j, half:, :] = extra
 
 
-def first_kernel(pos, x, before, gain, taps, mine, other, out, wb, w):
-    assemble(pos, mine, other, w)
+def first_kernel(x, before, gain, taps, own, own_far, near, near_far, out, wb, w):
+    assemble((own, own_far, near, near_far), w)
     back_weights(w, wb)
     chunks, width = 16, x.shape[1] // 16
     def part(k):
@@ -116,8 +102,8 @@
     store_gated(gate(acc, taps[0]), out, True)
 
 
-def second_kernel(pos, x, gain, taps, mine, other, out, wb, w):
-    assemble(pos, mine, other, w)
+def second_kernel(x, gain, taps, own, own_far, near, near_far, out, wb, w):
+    assemble((own, own_far, near, near_far), w)
     back_weights(w, wb)
     chunks, width = x.shape[0], x.shape[2]
     squares = None
@@ -164,14 +150,14 @@
         outs[0][...] = new
 
 
-def call(kernel, out_shape, n_in, smem=False, scratch=(), flops=0, moved=0):
-    specs = ([SMEM] if smem else []) + [VMEM] * (n_in - int(smem))
+def call(kernel, out_shape, n_in, scratch=(), flops=0, moved=0):
     return pl.pallas_call(
         kernel,
         out_shape=out_shape,
-        in_specs=specs,
+        in_specs=[VMEM] * n_in,
         out_specs=jax.tree.map(lambda _: VMEM, out_shape),
         scratch_shapes=scratch,
+        compiler_params=pltpu.CompilerParams(vmem_limit_bytes=24 << 20),
         cost_estimate=pl.CostEstimate(flops=flops, bytes_accessed=moved, transcendentals=0),
     )
 
@@ -182,42 +168,49 @@
     )
 
 
-def gather_planes(block):
-    low = exchange(block, 12)
-    high = exchange(block, -12)
-    half = ROWS // 2
-    up = exchange(jnp.concatenate([block, high, low[:half]], axis=0), 4)
-    down = exchange(jnp.concatenate([block, low, high[half:]], axis=0), -4)
-    first, second = slice(0, ROWS), slice(ROWS, 2 * ROWS)
-    own = jnp.concatenate(
-        [up[first], block, low, high, down[first], up[second], down[second]]
-        + [up[2 * ROWS :], down[2 * ROWS :]],
+def swap_cores(block):
+    return lax.ppermute(block, "sp", [(i, i ^ 1) for i in range(64)])
+
+
+def gather_far(blocks):
+    groups = [[r + 8 * k for k in range(8)] for r in range(8)]
+    return lax.all_gather(
+        blocks, "sp", axis=1, tiled=True, axis_index_groups=groups
+    )
+
+
+def gather_near(own):
+    half = own.shape[0] // 2
+    own_far = swap_cores(own)
+    near = jnp.concatenate(
+        [
+            exchange(own, 1),
+            exchange(own, -1),
+            exchange(own[:half], 2),
+            exchange(own[half:], -2),
+        ],
         axis=0,
     )
-    a = exchange(own, 1)
-    b = exchange(own, -1)
-    c = exchange(own[: 4 * ROWS], 2)
-    d = exchange(own[ROWS : 5 * ROWS], -2)
-    mine = jnp.concatenate([own, a, b, c, d], axis=0)
-    other = lax.ppermute(mine, "sp", [(i, i ^ 1) for i in range(64)])
-    return mine, other
+    return own, own_far, near, swap_cores(near)
 
 
 def per_device(tokens, norm_gain, w_outer, w_inner, w_value, w_back, taps):
     count, width = tokens.shape
     feats = w_back.shape[2]
-    own = lax.axis_index("tp")
-    sp = lax.axis_index("sp")
-    pos = jnp.stack([sp // 2, sp % 2]).astype(jnp.int32)
+    rank = lax.axis_index("tp")
     tp = lax.axis_size("tp")
 
-    packed = pack(w_outer, w_inner, w_value, w_back)
+    layers, _, mix = w_outer.shape
+    packed = call(
+        pack_kernel, jax.ShapeDtypeStruct((layers, ROWS, 4 * mix), BF16), 4
+    )(w_outer, w_inner, w_value, w_back)
     before = lax.ppermute(tokens[count - HALO :], "sp", [(i, i + 1) for i in range(63)])
-    held = [gather_planes(block) for block in packed]
+    far = gather_far(packed)
+    held = [gather_near(far[layer]) for layer in range(layers)]
 
     rows = count + HALO
     resid = lax.dynamic_slice_in_dim(
-        jnp.concatenate([before, tokens], axis=0), own * feats, feats, 1
+        jnp.concatenate([before, tokens], axis=0), rank * feats, feats, 1
     )
     weights = pltpu.VMEM((width, 256), BF16)
     back_shape = jax.ShapeDtypeStruct((1024, 512), BF16)
@@ -229,8 +222,8 @@
     gated, back = call(
         first_kernel,
         [jax.ShapeDtypeStruct((tp, count // 2 + HALO, 128), BF16), back_shape],
-        7, True, [weights], flops, 8 << 20,
-    )(pos, tokens, before, norm_gain, taps, *held[0])
+        8, [weights], flops, 8 << 20,
+    )(tokens, before, norm_gain, taps, *held[0])
     whole = swap(gated)
     resid, spread = call(
         functools.partial(back_kernel, True),
@@ -238,19 +231,19 @@
             jax.ShapeDtypeStruct((rows, feats), BF16),
             jax.ShapeDtypeStruct((tp, rows, feats), BF16),
         ],
-        3, False, [], 2 * rows * 1024 * 512, 4 << 20,
+        3, [], 2 * rows * 1024 * 512, 4 << 20,
     )(whole, back, resid)
     current = swap(spread)
     gated, back = call(
         second_kernel,
         [jax.ShapeDtypeStruct((tp, count // 2, 128), BF16), back_shape],
-        6, True, [weights], flops, 8 << 20,
-    )(pos, current, norm_gain, taps, *held[1])
+        7, [weights], flops, 8 << 20,
+    )(current, norm_gain, taps, *held[1])
     whole = swap(gated)
     (result,) = call(
         functools.partial(back_kernel, False),
         [jax.ShapeDtypeStruct((count, feats), BF16)],
-        3, False, [], 2 * rows * 1024 * 512, 4 << 20,
+        3, [], 2 * rows * 1024 * 512, 4 << 20,
     )(whole, back, resid)
     return result
 

time: 233 us -> 174 us (0.75)
  the two profiles are of different devices: /device:TPU:1 before, /device:TPU:32 now
where the time goes in v2:
time: 174 us; the launch traced here: 173 us
  blocking collectives  73.1 us (42%)
  starting transfers between devices  47 us (27%)
  waiting for transfers between devices  35.8 us (21%)
  local copies, waits for them, and re-layouts  10.2 us (6%)
  Pallas kernels  6.36 us (4%)
    all_gather x1, blocking collectives, gather_far(): lax.all_gather(blocks, 'sp', axis=1, tiled=True, axis_index_groups=groups)  58.8 us
    ppermute x8, starting transfers between devices, exchange(): lax.ppermute(block, 'sp', [(i, (i + 2 * distance) % 64) for i in range(64)])  27.6 us
    all_to_all x1, blocking collectives, per_device(): whole = swap(gated)  14.3 us
    all_to_all x1, waiting for transfers between devices, per_device(): whole = swap(gated)  13.5 us
    unnamed x35, local copies, waits for them, and re-layouts  9.36 us
    all_to_all x1, waiting for transfers between devices, per_device(): current = swap(spread)  9.07 us
    ppermute x4, starting transfers between devices, swap_cores(): return lax.ppermute(block, 'sp', [(i, i ^ 1) for i in range(64)])  8.65 us
    ppermute x8, waiting for transfers between devices, exchange(): lax.ppermute(block, 'sp', [(i, (i + 2 * distance) % 64) for i in range(64)])  8.41 us
  transfers between devices with their start and end apart: 15, of which 8 were waited for; matrix products, arithmetic and copies ran while one was open for 1% of the time, Pallas kernels for 0%

profile of v2, /device:TPU:32, one launch (start us, length us, event | category | flops | bytes accessed | tf_op | source)
XLA Modules:
  0.0 172.8 jit_solution(5232793675458788214)
XLA Ops:
  3.2 58.8 %all_gather.3 = bf16[2,512,256]{2,1,0:T(8,128)(2,1)S(1)} all-gather(bf16[2,64,256]{2,1,0:T(8,128)(2,1)S(1)} %shard_map.73), channel_id=1, replica_groups={{0,128,256,384,512,640,768,896},{16,144,272,400,528,656,784,912},{32,16..., dimensions={1}, use_global_device_ids=true | all-gather | bytes 589824 | tf_op jit(solution)/shard_map/all_gather | solution.py:177
  62.0 1.9 %collective-permute-start.2 = (bf16[512,256]{1,0:T(8,128)(2,1)S(1)}, bf16[512,256]{1,0:T(8,128)(2,1)S(1)}, u32[]{:S(2)}, u32[]{:S(2)}) collective-permute-start(bf16[512,256]{1,0:T(8,128)(2,1)S(1)} %get-tuple-element.22.own), channel_id=1, source_target_pairs={{0,32},{16,48},{32,64},{48,80},{64,96},{80,112},{96,128},{112,144}... | collective-permute-start | bytes 786440 | tf_op jit(solution)/shard_map/ppermute | solution.py:166
  63.9 3.9 %collective-permute-start.3 = (bf16[512,256]{1,0:T(8,128)(2,1)S(1)}, bf16[512,256]{1,0:T(8,128)(2,1)S(1)}, u32[]{:S(2)}, u32[]{:S(2)}) collective-permute-start(bf16[512,256]{1,0:T(8,128)(2,1)S(1)} %get-tuple-element.22.own), channel_id=1, source_target_pairs={{0,992},{16,1008},{32,0},{48,16},{64,32},{80,48},{96,64},{112,80},... | collective-permute-start | bytes 786440 | tf_op jit(solution)/shard_map/ppermute | solution.py:166
  68.6 1.9 %collective-permute-start.4 = (bf16[256,256]{1,0:T(8,128)(2,1)S(1)}, bf16[256,256]{1,0:T(8,128)(2,1)S(1)}, u32[]{:S(2)}, u32[]{:S(2)}) collective-permute-start(bf16[256,256]{1,0:T(8,128)(2,1)S(1)} %get-tuple-element.20), channel_id=1, source_target_pairs={{0,64},{16,80},{32,96},{48,112},{64,128},{80,144},{96,160},{112,17... | collective-permute-start | bytes 393224 | tf_op jit(solution)/shard_map/ppermute | solution.py:166
  70.5 6.0 %collective-permute-start.5 = (bf16[256,256]{1,0:T(8,128)(2,1)S(1)}, bf16[256,256]{1,0:T(8,128)(2,1)S(1)}, u32[]{:S(2)}, u32[]{:S(2)}) collective-permute-start(bf16[256,256]{1,0:T(8,128)(2,1)S(1)} %get-tuple-element.19), channel_id=1, source_target_pairs={{0,960},{16,976},{32,992},{48,1008},{64,0},{80,16},{96,32},{112,48... | collective-permute-start | bytes 393224 | tf_op jit(solution)/shard_map/ppermute | solution.py:166
  76.6 2.3 %collective-permute-done.4 = bf16[256,256]{1,0:T(8,128)(2,1)S(1)} collective-permute-done((bf16[256,256]{1,0:T(8,128)(2,1)S(1)}, bf16[256,256]{1,0:T(8,128)(2,1)S(1)}, u32[]{:S(2)}, u32[]{:S(2)}) %collective-permute-start.4) | collective-permute-done | bytes 131104 | tf_op jit(solution)/shard_map/ppermute | solution.py:166
  80.1 1.9 %collective-permute-start.6 = (bf16[1536,256]{1,0:T(8,128)(2,1)S(1)}, bf16[1536,256]{1,0:T(8,128)(2,1)S(1)}, u32[]{:S(2)}, u32[]{:S(2)}) collective-permute-start(bf16[1536,256]{1,0:T(8,128)(2,1)S(1)} %constant_dynamic-update-slice_fusion.near), channel_id=1, source_target_pairs={{0,16},{16,0},{32,48},{48,32},{64,80},{80,64},{96,112},{112,96},{1... | collective-permute-start | bytes 2359304 | tf_op jit(solution)/shard_map/ppermute | solution.py:172
  82.0 2.4 %collective-permute-start.1 = (bf16[512,256]{1,0:T(8,128)(2,1)S(1)}, bf16[512,256]{1,0:T(8,128)(2,1)S(1)}, u32[]{:S(2)}, u32[]{:S(2)}) collective-permute-start(bf16[512,256]{1,0:T(8,128)(2,1)S(1)} %get-tuple-element.22.own), channel_id=1, source_target_pairs={{0,16},{16,0},{32,48},{48,32},{64,80},{80,64},{96,112},{112,96},{1... | collective-permute-start | bytes 786440 | tf_op jit(solution)/shard_map/ppermute | solution.py:172
  84.5 1.9 %collective-permute-start = (bf16[8,4096]{1,0:T(8,128)(2,1)S(1)}, bf16[8,4096]{1,0:T(8,128)(2,1)S(1)}, u32[]{:S(2)}, u32[]{:S(2)}) collective-permute-start(bf16[8,4096]{1,0:T(8,128)(2,1)S(1)} %slice.37), channel_id=1, source_target_pairs={{0,16},{16,32},{32,48},{48,64},{64,80},{80,96},{96,112},{112,128},... | collective-permute-start | bytes 196616 | tf_op jit(solution)/shard_map/ppermute | solution.py:207
  86.4 3.6 %collective-permute-done.before = bf16[8,4096]{1,0:T(8,128)(2,1)S(1)} collective-permute-done((bf16[8,4096]{1,0:T(8,128)(2,1)S(1)}, bf16[8,4096]{1,0:T(8,128)(2,1)S(1)}, u32[]{:S(2)}, u32[]{:S(2)}) %collective-permute-start) | collective-permute-done | bytes 65568 | tf_op jit(solution)/shard_map/ppermute | solution.py:207
  90.1 2.6 %shard_map.74 = (bf16[16,136,128]{2,1,0:T(8,128)(2,1)}, bf16[1024,512]{1,0:T(8,128)(2,1)S(1)}) custom-call(bf16[256,4096]{1,0:T(8,128)(2,1)S(1)} %copy-done, bf16[8,4096]{1,0:T(8,128)(2,1)S(1)} %collective-permute-done.before, f32[2,4096]{1,0:T(2,128)S(1)} %copy-done.8, f32[2,3,64]{2,1,0:T(4,128)S(1)} %copy.8.taps, ...), custom_call_target="tpu_custom_call" | custom-call | flops 553648128 | bytes 8388608 | tf_op jit(solution)/shard_map/pallas_call | solution.py:222
  93.6 5.2 %all-to-all-start = ((bf16[16,136,128]{2,1,0:T(8,128)(2,1)}), bf16[16,136,128]{2,1,0:T(8,128)(2,1)S(1)}, u32[]{:S(2)}, u32[]{:S(2)}) async-start(bf16[16,136,128]{2,1,0:T(8,128)(2,1)} %get-tuple-element.11), calls=%async_computation | async-start | bytes 1114112 | tf_op jit(solution)/shard_map/all_to_all | solution.py:227
  98.8 13.5 %all-to-all-done.gathered = bf16[16,136,128]{2,1,0:T(8,128)(2,1)S(1)} async-done(((bf16[16,136,128]{2,1,0:T(8,128)(2,1)}), bf16[16,136,128]{2,1,0:T(8,128)(2,1)S(1)}, u32[]{:S(2)}, u32[]{:S(2)}) %all-to-all-start) | async-done | bytes 557088 | tf_op jit(solution)/shard_map/all_to_all | solution.py:227
  116.3 3.7 %all-to-all-start.1 = ((bf16[16,264,256]{2,1,0:T(8,128)(2,1)}), bf16[16,264,256]{2,1,0:T(8,128)(2,1)S(1)}, u32[]{:S(2)}, u32[]{:S(2)}) async-start(bf16[16,264,256]{2,1,0:T(8,128)(2,1)} %copy-done.1), calls=%async_computation.1 | async-start | bytes 4325376 | tf_op jit(solution)/shard_map/all_to_all | solution.py:236
  120.0 2.0 %collective-permute-start.8 = (bf16[512,256]{1,0:T(8,128)(2,1)S(1)}, bf16[512,256]{1,0:T(8,128)(2,1)S(1)}, u32[]{:S(2)}, u32[]{:S(2)}) collective-permute-start(bf16[512,256]{1,0:T(8,128)(2,1)S(1)} %get-tuple-element.21.own), channel_id=1, source_target_pairs={{0,32},{16,48},{32,64},{48,80},{64,96},{80,112},{96,128},{112,144}... | collective-permute-start | bytes 786440 | tf_op jit(solution)/shard_map/ppermute | solution.py:166
  122.0 3.8 %collective-permute-start.9 = (bf16[512,256]{1,0:T(8,128)(2,1)S(1)}, bf16[512,256]{1,0:T(8,128)(2,1)S(1)}, u32[]{:S(2)}, u32[]{:S(2)}) collective-permute-start(bf16[512,256]{1,0:T(8,128)(2,1)S(1)} %get-tuple-element.21.own), channel_id=1, source_target_pairs={{0,992},{16,1008},{32,0},{48,16},{64,32},{80,48},{96,64},{112,80},... | collective-permute-start | bytes 786440 | tf_op jit(solution)/shard_map/ppermute | solution.py:166
  125.8 2.2 %collective-permute-start.10 = (bf16[256,256]{1,0:T(8,128)(2,1)}, bf16[256,256]{1,0:T(8,128)(2,1)S(1)}, u32[]{:S(2)}, u32[]{:S(2)}) collective-permute-start(bf16[256,256]{1,0:T(8,128)(2,1)} %get-tuple-element.18), channel_id=1, source_target_pairs={{0,64},{16,80},{32,96},{48,112},{64,128},{80,144},{96,160},{112,17... | collective-permute-start | bytes 393224 | tf_op jit(solution)/shard_map/ppermute | solution.py:166
  128.0 5.8 %collective-permute-start.11 = (bf16[256,256]{1,0:T(8,128)(2,1)}, bf16[256,256]{1,0:T(8,128)(2,1)S(1)}, u32[]{:S(2)}, u32[]{:S(2)}) collective-permute-start(bf16[256,256]{1,0:T(8,128)(2,1)} %get-tuple-element.17), channel_id=1, source_target_pairs={{0,960},{16,976},{32,992},{48,1008},{64,0},{80,16},{96,32},{112,48... | collective-permute-start | bytes 393224 | tf_op jit(solution)/shard_map/ppermute | solution.py:166
  133.9 3.7 %collective-permute-done.10 = bf16[256,256]{1,0:T(8,128)(2,1)S(1)} collective-permute-done((bf16[256,256]{1,0:T(8,128)(2,1)}, bf16[256,256]{1,0:T(8,128)(2,1)S(1)}, u32[]{:S(2)}, u32[]{:S(2)}) %collective-permute-start.10) | collective-permute-done | bytes 131104 | tf_op jit(solution)/shard_map/ppermute | solution.py:166
  138.9 1.9 %collective-permute-start.12 = (bf16[1536,256]{1,0:T(8,128)(2,1)S(1)}, bf16[1536,256]{1,0:T(8,128)(2,1)S(1)}, u32[]{:S(2)}, u32[]{:S(2)}) collective-permute-start(bf16[1536,256]{1,0:T(8,128)(2,1)S(1)} %constant_dynamic-update-slice_fusion.4.near), channel_id=1, source_target_pairs={{0,16},{16,0},{32,48},{48,32},{64,80},{80,64},{96,112},{112,96},{1... | collective-permute-start | bytes 2359304 | tf_op jit(solution)/shard_map/ppermute | solution.py:172
  140.8 2.4 %collective-permute-start.7 = (bf16[512,256]{1,0:T(8,128)(2,1)S(1)}, bf16[512,256]{1,0:T(8,128)(2,1)S(1)}, u32[]{:S(2)}, u32[]{:S(2)}) collective-permute-start(bf16[512,256]{1,0:T(8,128)(2,1)S(1)} %get-tuple-element.21.own), channel_id=1, source_target_pairs={{0,16},{16,0},{32,48},{48,32},{64,80},{80,64},{96,112},{112,96},{1... | collective-permute-start | bytes 786440 | tf_op jit(solution)/shard_map/ppermute | solution.py:172
  145.3 9.1 %all-to-all-done.1.x = bf16[16,264,256]{2,1,0:T(8,128)(2,1)S(1)} async-done(((bf16[16,264,256]{2,1,0:T(8,128)(2,1)}), bf16[16,264,256]{2,1,0:T(8,128)(2,1)S(1)}, u32[]{:S(2)}, u32[]{:S(2)}) %all-to-all-start.1) | async-done | bytes 2162720 | tf_op jit(solution)/shard_map/all_to_all | solution.py:236
  155.5 1.8 %shard_map.76 = (bf16[16,128,128]{2,1,0:T(8,128)(2,1)S(1)}, bf16[1024,512]{1,0:T(8,128)(2,1)S(1)}) custom-call(bf16[16,264,256]{2,1,0:T(8,128)(2,1)S(1)} %all-to-all-done.1.x, f32[2,4096]{1,0:T(2,128)S(1)} %copy-done.8, f32[2,3,64]{2,1,0:T(4,128)S(1)} %copy.8.taps, bf16[512,256]{1,0:T(8,128)(2,1)S(1)} %get-tuple-element.21.own, ...), custom_call_target="tpu_custom_call" | custom-call | flops 553648128 | bytes 8388608 | tf_op jit(solution)/shard_map/pallas_call | solution.py:237
  157.3 14.3 %all_to_all.15.gathered = bf16[16,128,128]{2,1,0:T(8,128)(2,1)S(1)} all-to-all(bf16[16,128,128]{2,1,0:T(8,128)(2,1)S(1)} %get-tuple-element.14), channel_id=1, replica_groups=mesh['sp'=64,'tp'=16] {'tp'}, dimensions={0} | all-to-all | bytes 1048576 | tf_op jit(solution)/shard_map/all_to_all | solution.py:242
  (54 shorter events, 15.7 us)
Async XLA Ops:
  3.1 81.3 %copy-start = (bf16[256,4096]{1,0:T(8,128)(2,1)S(1)}, bf16[256,4096]{1,0:T(8,128)(2,1)}, u32[]{:S(2)}) copy-start(bf16[256,4096]{1,0:T(8,128)(2,1)} %x.1) | copy-start | bytes 6291460
  3.1 83.2 %copy-start.13 = (f32[2,3,64]{2,0,1:T(2,128)S(1)}, f32[2,3,64]{2,0,1:T(2,128)}, u32[]{:S(2)}) copy-start(f32[2,3,64]{2,0,1:T(2,128)} %param.13) | copy-start | bytes 4612
  3.1 86.9 %copy-start.8 = (f32[2,4096]{1,0:T(2,128)S(1)}, f32[2,4096]{1,0:T(2,128)}, u32[]{:S(2)}) copy-start(f32[2,4096]{1,0:T(2,128)} %gain.3) | copy-start | bytes 98308
  62.0 14.6 %collective-permute-start.2 = (bf16[512,256]{1,0:T(8,128)(2,1)S(1)}, bf16[512,256]{1,0:T(8,128)(2,1)S(1)}, u32[]{:S(2)}, u32[]{:S(2)}) collective-permute-start(bf16[512,256]{1,0:T(8,128)(2,1)S(1)} %get-tuple-element.22.own), channel_id=1, source_target_pairs={{0,32},{16,48},{32,64},{48,80},{64,96},{80,112},{96,128},{112,144}... | collective-permute-start | bytes 786440 | tf_op jit(solution)/shard_map/ppermute | solution.py:166
  63.9 12.7 %collective-permute-start.3 = (bf16[512,256]{1,0:T(8,128)(2,1)S(1)}, bf16[512,256]{1,0:T(8,128)(2,1)S(1)}, u32[]{:S(2)}, u32[]{:S(2)}) collective-permute-start(bf16[512,256]{1,0:T(8,128)(2,1)S(1)} %get-tuple-element.22.own), channel_id=1, source_target_pairs={{0,992},{16,1008},{32,0},{48,16},{64,32},{80,48},{96,64},{112,80},... | collective-permute-start | bytes 786440 | tf_op jit(solution)/shard_map/ppermute | solution.py:166
  68.6 10.4 %collective-permute-start.4 = (bf16[256,256]{1,0:T(8,128)(2,1)S(1)}, bf16[256,256]{1,0:T(8,128)(2,1)S(1)}, u32[]{:S(2)}, u32[]{:S(2)}) collective-permute-start(bf16[256,256]{1,0:T(8,128)(2,1)S(1)} %get-tuple-element.20), channel_id=1, source_target_pairs={{0,64},{16,80},{32,96},{48,112},{64,128},{80,144},{96,160},{112,17... | collective-permute-start | bytes 393224 | tf_op jit(solution)/shard_map/ppermute | solution.py:166
  70.5 9.6 %collective-permute-start.5 = (bf16[256,256]{1,0:T(8,128)(2,1)S(1)}, bf16[256,256]{1,0:T(8,128)(2,1)S(1)}, u32[]{:S(2)}, u32[]{:S(2)}) collective-permute-start(bf16[256,256]{1,0:T(8,128)(2,1)S(1)} %get-tuple-element.19), channel_id=1, source_target_pairs={{0,960},{16,976},{32,992},{48,1008},{64,0},{80,16},{96,32},{112,48... | collective-permute-start | bytes 393224 | tf_op jit(solution)/shard_map/ppermute | solution.py:166
  80.1 10.0 %collective-permute-start.6 = (bf16[1536,256]{1,0:T(8,128)(2,1)S(1)}, bf16[1536,256]{1,0:T(8,128)(2,1)S(1)}, u32[]{:S(2)}, u32[]{:S(2)}) collective-permute-start(bf16[1536,256]{1,0:T(8,128)(2,1)S(1)} %constant_dynamic-update-slice_fusion.near), channel_id=1, source_target_pairs={{0,16},{16,0},{32,48},{48,32},{64,80},{80,64},{96,112},{112,96},{1... | collective-permute-start | bytes 2359304 | tf_op jit(solution)/shard_map/ppermute | solution.py:172
  82.0 8.0 %collective-permute-start.1 = (bf16[512,256]{1,0:T(8,128)(2,1)S(1)}, bf16[512,256]{1,0:T(8,128)(2,1)S(1)}, u32[]{:S(2)}, u32[]{:S(2)}) collective-permute-start(bf16[512,256]{1,0:T(8,128)(2,1)S(1)} %get-tuple-element.22.own), channel_id=1, source_target_pairs={{0,16},{16,0},{32,48},{48,32},{64,80},{80,64},{96,112},{112,96},{1... | collective-permute-start | bytes 786440 | tf_op jit(solution)/shard_map/ppermute | solution.py:172
  84.5 5.6 %collective-permute-start = (bf16[8,4096]{1,0:T(8,128)(2,1)S(1)}, bf16[8,4096]{1,0:T(8,128)(2,1)S(1)}, u32[]{:S(2)}, u32[]{:S(2)}) collective-permute-start(bf16[8,4096]{1,0:T(8,128)(2,1)S(1)} %slice.37), channel_id=1, source_target_pairs={{0,16},{16,32},{32,48},{48,64},{64,80},{80,96},{96,112},{112,128},... | collective-permute-start | bytes 196616 | tf_op jit(solution)/shard_map/ppermute | solution.py:207
  92.6 1.0 copy-start.2
  93.6 18.7 %all-to-all-start = ((bf16[16,136,128]{2,1,0:T(8,128)(2,1)}), bf16[16,136,128]{2,1,0:T(8,128)(2,1)S(1)}, u32[]{:S(2)}, u32[]{:S(2)}) async-start(bf16[16,136,128]{2,1,0:T(8,128)(2,1)} %get-tuple-element.11), calls=%async_computation | async-start | bytes 1114112 | tf_op jit(solution)/shard_map/all_to_all | solution.py:227
  112.3 1.2 copy-start.3
  114.2 1.4 copy-start.1
  116.3 38.1 %all-to-all-start.1 = ((bf16[16,264,256]{2,1,0:T(8,128)(2,1)}), bf16[16,264,256]{2,1,0:T(8,128)(2,1)S(1)}, u32[]{:S(2)}, u32[]{:S(2)}) async-start(bf16[16,264,256]{2,1,0:T(8,128)(2,1)} %copy-done.1), calls=%async_computation.1 | async-start | bytes 4325376 | tf_op jit(solution)/shard_map/all_to_all | solution.py:236
  120.0 13.8 %collective-permute-start.8 = (bf16[512,256]{1,0:T(8,128)(2,1)S(1)}, bf16[512,256]{1,0:T(8,128)(2,1)S(1)}, u32[]{:S(2)}, u32[]{:S(2)}) collective-permute-start(bf16[512,256]{1,0:T(8,128)(2,1)S(1)} %get-tuple-element.21.own), channel_id=1, source_target_pairs={{0,32},{16,48},{32,64},{48,80},{64,96},{80,112},{96,128},{112,144}... | collective-permute-start | bytes 786440 | tf_op jit(solution)/shard_map/ppermute | solution.py:166
  122.0 11.8 %collective-permute-start.9 = (bf16[512,256]{1,0:T(8,128)(2,1)S(1)}, bf16[512,256]{1,0:T(8,128)(2,1)S(1)}, u32[]{:S(2)}, u32[]{:S(2)}) collective-permute-start(bf16[512,256]{1,0:T(8,128)(2,1)S(1)} %get-tuple-element.21.own), channel_id=1, source_target_pairs={{0,992},{16,1008},{32,0},{48,16},{64,32},{80,48},{96,64},{112,80},... | collective-permute-start | bytes 786440 | tf_op jit(solution)/shard_map/ppermute | solution.py:166
  125.8 11.7 %collective-permute-start.10 = (bf16[256,256]{1,0:T(8,128)(2,1)}, bf16[256,256]{1,0:T(8,128)(2,1)S(1)}, u32[]{:S(2)}, u32[]{:S(2)}) collective-permute-start(bf16[256,256]{1,0:T(8,128)(2,1)} %get-tuple-element.18), channel_id=1, source_target_pairs={{0,64},{16,80},{32,96},{48,112},{64,128},{80,144},{96,160},{112,17... | collective-permute-start | bytes 393224 | tf_op jit(solution)/shard_map/ppermute | solution.py:166
  128.0 10.9 %collective-permute-start.11 = (bf16[256,256]{1,0:T(8,128)(2,1)}, bf16[256,256]{1,0:T(8,128)(2,1)S(1)}, u32[]{:S(2)}, u32[]{:S(2)}) collective-permute-start(bf16[256,256]{1,0:T(8,128)(2,1)} %get-tuple-element.17), channel_id=1, source_target_pairs={{0,960},{16,976},{32,992},{48,1008},{64,0},{80,16},{96,32},{112,48... | collective-permute-start | bytes 393224 | tf_op jit(solution)/shard_map/ppermute | solution.py:166
  138.9 5.5 %collective-permute-start.12 = (bf16[1536,256]{1,0:T(8,128)(2,1)S(1)}, bf16[1536,256]{1,0:T(8,128)(2,1)S(1)}, u32[]{:S(2)}, u32[]{:S(2)}) collective-permute-start(bf16[1536,256]{1,0:T(8,128)(2,1)S(1)} %constant_dynamic-update-slice_fusion.4.near), channel_id=1, source_target_pairs={{0,16},{16,0},{32,48},{48,32},{64,80},{80,64},{96,112},{112,96},{1... | collective-permute-start | bytes 2359304 | tf_op jit(solution)/shard_map/ppermute | solution.py:172
  140.8 3.6 %collective-permute-start.7 = (bf16[512,256]{1,0:T(8,128)(2,1)S(1)}, bf16[512,256]{1,0:T(8,128)(2,1)S(1)}, u32[]{:S(2)}, u32[]{:S(2)}) collective-permute-start(bf16[512,256]{1,0:T(8,128)(2,1)S(1)} %get-tuple-element.21.own), channel_id=1, source_target_pairs={{0,16},{16,0},{32,48},{48,32},{64,80},{80,64},{96,112},{112,96},{1... | collective-permute-start | bytes 786440 | tf_op jit(solution)/shard_map/ppermute | solution.py:172
  144.4 0.9 copy-start.4
  154.3 1.1 copy-start.5
  155.5 16.1 %copy-start.7 = (bf16[264,256]{1,0:T(8,128)(2,1)S(1)}, bf16[264,256]{1,0:T(8,128)(2,1)}, u32[]{:S(2)}) copy-start(bf16[264,256]{1,0:T(8,128)(2,1)} %copy-done.6) | copy-start | bytes 405508
  (5 other events, 3.6 us)

commit v3 on v2

--- a/solution.py
+++ b/solution.py
@@ -7,6 +7,7 @@
 from jax.experimental.pallas import tpu as pltpu
 from jax.sharding import PartitionSpec as P
 
+
 EPS = 1e-06
 HALO = 8
 ROWS = 64
@@ -15,36 +16,61 @@
 F32 = jnp.float32
 
 
-def pack_kernel(wo, wi, wv, wb, out):
+def pack_kernel(*refs):
+    sources, (out, *held, sems) = refs[:4], refs[4:]
+    copies = [
+        pltpu.make_async_copy(src, dst, sems.at[i])
+        for i, (src, dst) in enumerate(zip(sources, held))
+    ]
+    for copy in copies:
+        copy.start()
+    for copy in copies:
+        copy.wait()
     for layer in range(out.shape[0]):
-        back = wb[layer].astype(F32)
+        back = held[3][layer].astype(F32)
         columns = back.shape[1] // 4
         folded = jnp.concatenate(
             [back[:, k * columns : (k + 1) * columns] for k in range(4)], axis=0
         )
-        parts = [w[layer].astype(F32) for w in (wo, wi, wv)] + [folded]
+        parts = [w[layer].astype(F32) for w in held[:3]] + [folded]
         out[layer] = jnp.concatenate(parts, axis=1).astype(BF16)
 
 
+def pack(*arrays):
+    layers, _, mix = arrays[0].shape
+    return pl.pallas_call(
+        pack_kernel,
+        out_shape=jax.ShapeDtypeStruct((layers, ROWS, 4 * mix), BF16),
+        in_specs=[pl.BlockSpec(memory_space=pltpu.HBM)] * 4,
+        out_specs=VMEM,
+        scratch_shapes=[pltpu.VMEM(a.shape, a.dtype) for a in arrays]
+        + [pltpu.SemaphoreType.DMA((4,))],
+    )(*arrays)
+
+
 def assemble(blocks, w):
-    own, own_far, near, near_far = blocks
     sp = lax.axis_index("sp")
     plane, core = lax.rem(lax.div(sp, 2), 4), lax.rem(sp, 2)
-    for shift, part, count in ((0, None, 8), (3, 0, 8), (1, 8, 8), (2, 16, 8)):
-        residue = lax.rem(plane + shift, 4)
-        for side, (first, rest) in enumerate(((own, near), (own_far, near_far))):
-            start = 128 * residue + 64 * (core if side == 0 else 1 - core)
-            for k in range(count):
-                source = first if part is None else rest
-                at = (k if part is None else part + k) * ROWS
+    far = 1 - core
+    down, up = 3 - 2 * core, 1 + 2 * core
+    places = (
+        ((0, core), (0, far)),
+        ((down, core), (down, far), (2, core)),
+        ((up, far), (up, core), (2, far)),
+    )
+    for block, parts in zip(blocks, places):
+        for p, (shift, side) in enumerate(parts):
+            start = 128 * lax.rem(plane + shift, 4) + 64 * side
+            for k in range(8):
+                at = (8 * p + k) * ROWS
                 row = pl.multiple_of(512 * k + start, 64)
-                w[pl.ds(row, ROWS), :] = source[at : at + ROWS, :]
+                w[pl.ds(row, ROWS), :] = block[at : at + ROWS, :]
 
 
 def back_weights(w, wb):
     whole = w[:, 128:].reshape(64, 4, 16, 128)
-    for k in range(4):
-        wb[:, k * 128 : (k + 1) * 128] = whole[:, k].reshape(1024, 128)
+    parts = [whole[:, k].reshape(1024, 128)[:, 64:] for k in range(4)]
+    wb[...] = jnp.concatenate(parts, axis=1)
 
 
 def rounded(v):
@@ -78,8 +104,8 @@
             out[j, half:, :] = extra
 
 
-def first_kernel(x, before, gain, taps, own, own_far, near, near_far, out, wb, w):
-    assemble((own, own_far, near, near_far), w)
+def first_kernel(x, before, gain, taps, own, near, near_far, out, wb, w):
+    assemble((own, near, near_far), w)
     back_weights(w, wb)
     chunks, width = 16, x.shape[1] // 16
     def part(k):
@@ -102,8 +128,8 @@
     store_gated(gate(acc, taps[0]), out, True)
 
 
-def second_kernel(x, gain, taps, own, own_far, near, near_far, out, wb, w):
-    assemble((own, own_far, near, near_far), w)
+def second_kernel(x, gain, taps, own, near, near_far, out, wb, w):
+    assemble((own, near, near_far), w)
     back_weights(w, wb)
     chunks, width = x.shape[0], x.shape[2]
     squares = None
@@ -136,10 +162,7 @@
             rows = [jnp.concatenate([a[half:, :64], b[half:, :64]], axis=1)] + rows
         lefts.append(jnp.concatenate(rows, axis=0).astype(BF16))
     left = jnp.concatenate(lefts, axis=1)
-    wide = jnp.dot(left, wb[...], preferred_element_type=F32)
-    proj = jnp.concatenate(
-        [wide[:, k * 128 + 64 : (k + 1) * 128] for k in range(4)], axis=1
-    )
+    proj = jnp.dot(left, wb[...], preferred_element_type=F32)
     start = resid.shape[0] - proj.shape[0]
     new = (resid[...].astype(F32)[start:] + proj).astype(BF16)
     if halo:
@@ -163,9 +186,8 @@
 
 
 def exchange(block, distance):
-    return lax.ppermute(
-        block, "sp", [(i, (i + 2 * distance) % 64) for i in range(64)]
-    )
+    step = [2 * distance, -2 * distance]
+    return lax.ppermute(block, "sp", [(i, (i + step[i % 2]) % 64) for i in range(64)])
 
 
 def swap_cores(block):
@@ -177,21 +199,6 @@
     return lax.all_gather(
         blocks, "sp", axis=1, tiled=True, axis_index_groups=groups
     )
-
-
-def gather_near(own):
-    half = own.shape[0] // 2
-    own_far = swap_cores(own)
-    near = jnp.concatenate(
-        [
-            exchange(own, 1),
-            exchange(own, -1),
-            exchange(own[:half], 2),
-            exchange(own[half:], -2),
-        ],
-        axis=0,
-    )
-    return own, own_far, near, swap_cores(near)
 
 
 def per_device(tokens, norm_gain, w_outer, w_inner, w_value, w_back, taps):
@@ -199,51 +206,60 @@
     feats = w_back.shape[2]
     rank = lax.axis_index("tp")
     tp = lax.axis_size("tp")
-
-    layers, _, mix = w_outer.shape
-    packed = call(
-        pack_kernel, jax.ShapeDtypeStruct((layers, ROWS, 4 * mix), BF16), 4
-    )(w_outer, w_inner, w_value, w_back)
+    layers = w_outer.shape[0]
+    rows = count + HALO
+
+    packed = pack(w_outer, w_inner, w_value, w_back)
     before = lax.ppermute(tokens[count - HALO :], "sp", [(i, i + 1) for i in range(63)])
     far = gather_far(packed)
-    held = [gather_near(far[layer]) for layer in range(layers)]
-
-    rows = count + HALO
-    resid = lax.dynamic_slice_in_dim(
-        jnp.concatenate([before, tokens], axis=0), rank * feats, feats, 1
-    )
+    twos = []
+    for layer in range(layers):
+        twos.append(exchange(far[layer], 2))
+    partner = swap_cores(far)
+    held = []
+    for layer in range(layers):
+        both = jnp.concatenate([far[layer], partner[layer]], axis=0)
+        one = exchange(both, 1)
+        near = jnp.concatenate([one, twos[layer]], axis=0)
+        if layer == 0:
+            resid = lax.dynamic_slice_in_dim(
+                jnp.concatenate([before, tokens], axis=0), rank * feats, feats, 1
+            )
+            near, before, resid = lax.optimization_barrier((near, before, resid))
+        held.append((both, near, swap_cores(near)))
+
     weights = pltpu.VMEM((width, 256), BF16)
-    back_shape = jax.ShapeDtypeStruct((1024, 512), BF16)
+    back_shape = jax.ShapeDtypeStruct((1024, 256), BF16)
     flops = 2 * rows * width * 256
-    swap = functools.partial(
+    send = functools.partial(
         lax.all_to_all, axis_name="tp", split_axis=0, concat_axis=0, tiled=True
     )
 
     gated, back = call(
         first_kernel,
         [jax.ShapeDtypeStruct((tp, count // 2 + HALO, 128), BF16), back_shape],
-        8, [weights], flops, 8 << 20,
+        7, [weights], flops, 8 << 20,
     )(tokens, before, norm_gain, taps, *held[0])
-    whole = swap(gated)
+    whole = send(gated)
     resid, spread = call(
         functools.partial(back_kernel, True),
         [
             jax.ShapeDtypeStruct((rows, feats), BF16),
             jax.ShapeDtypeStruct((tp, rows, feats), BF16),
         ],
-        3, [], 2 * rows * 1024 * 512, 4 << 20,
+        3, [], 2 * rows * 1024 * 256, 4 << 20,
     )(whole, back, resid)
-    current = swap(spread)
+    current = send(spread)
     gated, back = call(
         second_kernel,
         [jax.ShapeDtypeStruct((tp, count // 2, 128), BF16), back_shape],
-        7, [weights], flops, 8 << 20,
+        6, [weights], flops, 8 << 20,
     )(current, norm_gain, taps, *held[1])
-    whole = swap(gated)
+    whole = send(gated)
     (result,) = call(
         functools.partial(back_kernel, False),
         [jax.ShapeDtypeStruct((count, feats), BF16)],
-        3, [], 2 * rows * 1024 * 512, 4 << 20,
+        3, [], 2 * rows * 1024 * 256, 4 << 20,
     )(whole, back, resid)
     return result
 

time: 174 us -> 162 us (0.931)
  the two profiles are of different devices: /device:TPU:32 before, /device:TPU:1 now
where the time goes in v3:
time: 162 us
  blocking collectives  85.4 us (53%)
  starting transfers between devices  34.4 us (21%)
  waiting for transfers between devices  27.6 us (17%)
  Pallas kernels  6.41 us (4%)
  local copies, waits for them, and re-layouts  5.5 us (3%)
  other arithmetic  2.13 us (1%)
    all_gather x1, blocking collectives, gather_far(): lax.all_gather(blocks, 'sp', axis=1, tiled=True, axis_index_groups=groups)  53 us
    all_to_all x2, blocking collectives, per_device(): whole = send(gated)  32.4 us
    ppermute x3, starting transfers between devices, swap_cores(): return lax.ppermute(block, 'sp', [(i, i ^ 1) for i in range(64)])  15.3 us
    ppermute x4, waiting for transfers between devices, exchange(): lax.ppermute(block, 'sp', [(i, (i + step[i % 2]) % 64) for i in range(64)])  14.6 us
    ppermute x4, starting transfers between devices, exchange(): lax.ppermute(block, 'sp', [(i, (i + step[i % 2]) % 64) for i in range(64)])  12.2 us
    all_to_all x1, waiting for transfers between devices, per_device(): current = send(spread)  6.35 us
    ppermute x3, waiting for transfers between devices, swap_cores(): return lax.ppermute(block, 'sp', [(i, i ^ 1) for i in range(64)])  4.53 us
    unnamed x18, local copies, waits for them, and re-layouts  4.07 us
  transfers between devices with their start and end apart: 9, of which 8 were waited for; matrix products, arithmetic and copies ran while one was open for 2% of the time, Pallas kernels for 0%

profile of v3, /device:TPU:1, one launch (start us, length us, event | category | flops | bytes accessed | tf_op | source)
XLA Modules:
  0.0 161.7 jit_solution(8224808404484914865)
XLA Ops:
  0.0 1.7 %shard_map.73 = bf16[2,64,256]{2,1,0:T(8,128)(2,1)} custom-call(bf16[2,64,64]{2,1,0:T(8,128)(2,1)} %refs_0_.1, bf16[2,64,64]{2,1,0:T(8,128)(2,1)} %refs_1_.1, bf16[2,64,64]{2,1,0:T(8,128)(2,1)} %refs_2_.1, bf16[2,16,256]{2,1,0:T(8,128)(2,1)} %refs_3_.1), custom_call_target="tpu_custom_call" | custom-call | tf_op jit(solution)/shard_map/pallas_call | solution.py:41
  1.8 53.0 %all_gather.3 = bf16[2,512,256]{2,1,0:T(8,128)(2,1)S(1)} all-gather(bf16[2,64,256]{2,1,0:T(8,128)(2,1)} %shard_map.73), channel_id=1, replica_groups={{0,128,256,384,512,640,768,896},{16,144,272,400,528,656,784,912},{32,16..., dimensions={1}, use_global_device_ids=true | all-gather | bytes 589824 | tf_op jit(solution)/shard_map/all_gather | solution.py:199
  54.7 9.0 %collective-permute-start = (bf16[2,512,256]{2,1,0:T(8,128)(2,1)S(1)}, bf16[2,512,256]{2,1,0:T(8,128)(2,1)S(1)}, u32[]{:S(2)}, u32[]{:S(2)}) collective-permute-start(bf16[2,512,256]{2,1,0:T(8,128)(2,1)S(1)} %all_gather.3), channel_id=1, source_target_pairs={{0,16},{16,0},{32,48},{48,32},{64,80},{80,64},{96,112},{112,96},{1... | collective-permute-start | bytes 1572872 | tf_op jit(solution)/shard_map/ppermute | solution.py:194
  65.4 2.8 %collective-permute-start.1 = (bf16[1024,256]{1,0:T(8,128)(2,1)S(1)}, bf16[1024,256]{1,0:T(8,128)(2,1)}, u32[]{:S(2)}, u32[]{:S(2)}) collective-permute-start(bf16[1024,256]{1,0:T(8,128)(2,1)S(1)} %pad_maximum_fusion.1.own), channel_id=1, source_target_pairs={{0,32},{16,1008},{32,64},{48,16},{64,96},{80,48},{96,128},{112,80}... | collective-permute-start | bytes 1572872 | tf_op jit(solution)/shard_map/ppermute | solution.py:190
  68.2 1.9 %collective-permute-start.2 = (bf16[512,256]{1,0:T(8,128)(2,1)S(1)}, bf16[512,256]{1,0:T(8,128)(2,1)S(1)}, u32[]{:S(2)}, u32[]{:S(2)}) collective-permute-start(bf16[512,256]{1,0:T(8,128)(2,1)S(1)} %get-tuple-element.24), channel_id=1, source_target_pairs={{0,64},{16,976},{32,96},{48,1008},{64,128},{80,16},{96,160},{112,4... | collective-permute-start | bytes 786440 | tf_op jit(solution)/shard_map/ppermute | solution.py:190
  70.7 3.2 %collective-permute-start.3 = (bf16[8,4096]{1,0:T(8,128)(2,1)}, bf16[8,4096]{1,0:T(8,128)(2,1)S(1)}, u32[]{:S(2)}, u32[]{:S(2)}) collective-permute-start(bf16[8,4096]{1,0:T(8,128)(2,1)} %slice.19), channel_id=1, source_target_pairs={{0,16},{16,32},{32,48},{48,64},{64,80},{80,96},{96,112},{112,128},... | collective-permute-start | bytes 196616 | tf_op jit(solution)/shard_map/ppermute | solution.py:213
  74.0 2.2 %collective-permute-done.3.before = bf16[8,4096]{1,0:T(8,128)(2,1)S(1)} collective-permute-done((bf16[8,4096]{1,0:T(8,128)(2,1)}, bf16[8,4096]{1,0:T(8,128)(2,1)S(1)}, u32[]{:S(2)}, u32[]{:S(2)}) %collective-permute-start.3) | collective-permute-done | bytes 65568 | tf_op jit(solution)/shard_map/ppermute | solution.py:213
  76.2 6.7 %collective-permute-done.2 = bf16[512,256]{1,0:T(8,128)(2,1)S(1)} collective-permute-done((bf16[512,256]{1,0:T(8,128)(2,1)S(1)}, bf16[512,256]{1,0:T(8,128)(2,1)S(1)}, u32[]{:S(2)}, u32[]{:S(2)}) %collective-permute-start.2) | collective-permute-done | bytes 262176 | tf_op jit(solution)/shard_map/ppermute | solution.py:190
  84.0 2.8 %collective-permute-start.4 = (bf16[1536,256]{1,0:T(8,128)(2,1)S(1)}, bf16[1536,256]{1,0:T(8,128)(2,1)S(1)}, u32[]{:S(2)}, u32[]{:S(2)}) collective-permute-start(bf16[1536,256]{1,0:T(8,128)(2,1)S(1)} %pad_maximum_fusion.near), channel_id=1, source_target_pairs={{0,16},{16,0},{32,48},{48,32},{64,80},{80,64},{96,112},{112,96},{1... | collective-permute-start | bytes 2359304 | tf_op jit(solution)/shard_map/ppermute | solution.py:194
  86.8 1.9 %collective-permute-done.4.near_far = bf16[1536,256]{1,0:T(8,128)(2,1)S(1)} collective-permute-done((bf16[1536,256]{1,0:T(8,128)(2,1)S(1)}, bf16[1536,256]{1,0:T(8,128)(2,1)S(1)}, u32[]{:S(2)}, u32[]{:S(2)}) %collective-permute-start.4) | collective-permute-done | bytes 786464 | tf_op jit(solution)/shard_map/ppermute | solution.py:194
  88.7 1.6 shard_map.74
  90.3 16.4 %all_to_all.15.gathered = bf16[16,136,128]{2,1,0:T(8,128)(2,1)S(1)} all-to-all(bf16[16,136,128]{2,1,0:T(8,128)(2,1)S(1)} %get-tuple-element.16), channel_id=1, replica_groups=mesh['sp'=64,'tp'=16] {'tp'}, dimensions={0} | all-to-all | bytes 1114112 | tf_op jit(solution)/shard_map/all_to_all | solution.py:243
  107.1 1.3 copy-done.1
  109.1 3.7 %all-to-all-start.1 = ((bf16[16,264,256]{2,1,0:T(8,128)(2,1)}), bf16[16,264,256]{2,1,0:T(8,128)(2,1)S(1)}, u32[]{:S(2)}, u32[]{:S(2)}) async-start(bf16[16,264,256]{2,1,0:T(8,128)(2,1)} %copy-done.1), calls=%async_computation.1 | async-start | bytes 4325376 | tf_op jit(solution)/shard_map/all_to_all | solution.py:252
  113.9 1.9 %collective-permute-start.5 = (bf16[1024,256]{1,0:T(8,128)(2,1)S(1)}, bf16[1024,256]{1,0:T(8,128)(2,1)S(1)}, u32[]{:S(2)}, u32[]{:S(2)}) collective-permute-start(bf16[1024,256]{1,0:T(8,128)(2,1)S(1)} %pad_maximum_fusion.2.own), channel_id=1, source_target_pairs={{0,32},{16,1008},{32,64},{48,16},{64,96},{80,48},{96,128},{112,80}... | collective-permute-start | bytes 1572872 | tf_op jit(solution)/shard_map/ppermute | solution.py:190
  115.8 5.6 %collective-permute-start.6 = (bf16[512,256]{1,0:T(8,128)(2,1)}, bf16[512,256]{1,0:T(8,128)(2,1)S(1)}, u32[]{:S(2)}, u32[]{:S(2)}) collective-permute-start(bf16[512,256]{1,0:T(8,128)(2,1)} %get-tuple-element.23), channel_id=1, source_target_pairs={{0,64},{16,976},{32,96},{48,1008},{64,128},{80,16},{96,160},{112,4... | collective-permute-start | bytes 786440 | tf_op jit(solution)/shard_map/ppermute | solution.py:190
  121.4 2.7 %collective-permute-done.5 = bf16[1024,256]{1,0:T(8,128)(2,1)S(1)} collective-permute-done((bf16[1024,256]{1,0:T(8,128)(2,1)S(1)}, bf16[1024,256]{1,0:T(8,128)(2,1)S(1)}, u32[]{:S(2)}, u32[]{:S(2)}) %collective-permute-start.5) | collective-permute-done | bytes 524320 | tf_op jit(solution)/shard_map/ppermute | solution.py:190
  124.1 5.2 %collective-permute-done.6 = bf16[512,256]{1,0:T(8,128)(2,1)S(1)} collective-permute-done((bf16[512,256]{1,0:T(8,128)(2,1)}, bf16[512,256]{1,0:T(8,128)(2,1)S(1)}, u32[]{:S(2)}, u32[]{:S(2)}) %collective-permute-start.6) | collective-permute-done | bytes 262176 | tf_op jit(solution)/shard_map/ppermute | solution.py:190
  129.3 3.4 %collective-permute-start.7 = (bf16[1536,256]{1,0:T(8,128)(2,1)S(1)}, bf16[1536,256]{1,0:T(8,128)(2,1)S(1)}, u32[]{:S(2)}, u32[]{:S(2)}) collective-permute-start(bf16[1536,256]{1,0:T(8,128)(2,1)S(1)} %constant_dynamic-update-slice_fusion.near), channel_id=1, source_target_pairs={{0,16},{16,0},{32,48},{48,32},{64,80},{80,64},{96,112},{112,96},{1... | collective-permute-start | bytes 2359304 | tf_op jit(solution)/shard_map/ppermute | solution.py:194
  132.7 1.9 %collective-permute-done.7.near_far = bf16[1536,256]{1,0:T(8,128)(2,1)S(1)} collective-permute-done((bf16[1536,256]{1,0:T(8,128)(2,1)S(1)}, bf16[1536,256]{1,0:T(8,128)(2,1)S(1)}, u32[]{:S(2)}, u32[]{:S(2)}) %collective-permute-start.7) | collective-permute-done | bytes 786464 | tf_op jit(solution)/shard_map/ppermute | solution.py:194
  135.5 6.3 %all-to-all-done.1.x = bf16[16,264,256]{2,1,0:T(8,128)(2,1)S(1)} async-done(((bf16[16,264,256]{2,1,0:T(8,128)(2,1)}), bf16[16,264,256]{2,1,0:T(8,128)(2,1)S(1)}, u32[]{:S(2)}, u32[]{:S(2)}) %all-to-all-start.1) | async-done | bytes 2162720 | tf_op jit(solution)/shard_map/all_to_all | solution.py:252
  141.9 1.1 copy-done.3
  143.0 1.6 shard_map.76
  144.6 16.0 %all_to_all.16.gathered = bf16[16,128,128]{2,1,0:T(8,128)(2,1)S(1)} all-to-all(bf16[16,128,128]{2,1,0:T(8,128)(2,1)S(1)} %get-tuple-element.20), channel_id=1, replica_groups=mesh['sp'=64,'tp'=16] {'tp'}, dimensions={0} | all-to-all | bytes 1048576 | tf_op jit(solution)/shard_map/all_to_all | solution.py:258
  (28 shorter events, 7.4 us)
Async XLA Ops:
  0.0 70.1 %copy-start = (bf16[256,4096]{1,0:T(8,128)(2,1)S(1)}, bf16[256,4096]{1,0:T(8,128)(2,1)}, u32[]{:S(2)}) copy-start(bf16[256,4096]{1,0:T(8,128)(2,1)} %x.1) | copy-start | bytes 6291460
  54.7 10.6 %collective-permute-start = (bf16[2,512,256]{2,1,0:T(8,128)(2,1)S(1)}, bf16[2,512,256]{2,1,0:T(8,128)(2,1)S(1)}, u32[]{:S(2)}, u32[]{:S(2)}) collective-permute-start(bf16[2,512,256]{2,1,0:T(8,128)(2,1)S(1)} %all_gather.3), channel_id=1, source_target_pairs={{0,16},{16,0},{32,48},{48,32},{64,80},{80,64},{96,112},{112,96},{1... | collective-permute-start | bytes 1572872 | tf_op jit(solution)/shard_map/ppermute | solution.py:194
  65.4 21.4 %copy-start.7 = (f32[2,3,64]{2,0,1:T(2,128)S(1)}, f32[2,3,64]{2,0,1:T(2,128)}, u32[]{:S(2)}) copy-start(f32[2,3,64]{2,0,1:T(2,128)} %param.13) | copy-start | bytes 4612
  65.4 23.3 %copy-start.6 = (f32[2,4096]{1,0:T(2,128)S(1)}, f32[2,4096]{1,0:T(2,128)}, u32[]{:S(2)}) copy-start(f32[2,4096]{1,0:T(2,128)} %gain.3) | copy-start | bytes 98308
  65.4 17.5 %collective-permute-start.1 = (bf16[1024,256]{1,0:T(8,128)(2,1)S(1)}, bf16[1024,256]{1,0:T(8,128)(2,1)}, u32[]{:S(2)}, u32[]{:S(2)}) collective-permute-start(bf16[1024,256]{1,0:T(8,128)(2,1)S(1)} %pad_maximum_fusion.1.own), channel_id=1, source_target_pairs={{0,32},{16,1008},{32,64},{48,16},{64,96},{80,48},{96,128},{112,80}... | collective-permute-start | bytes 1572872 | tf_op jit(solution)/shard_map/ppermute | solution.py:190
  68.2 14.7 %collective-permute-start.2 = (bf16[512,256]{1,0:T(8,128)(2,1)S(1)}, bf16[512,256]{1,0:T(8,128)(2,1)S(1)}, u32[]{:S(2)}, u32[]{:S(2)}) collective-permute-start(bf16[512,256]{1,0:T(8,128)(2,1)S(1)} %get-tuple-element.24), channel_id=1, source_target_pairs={{0,64},{16,976},{32,96},{48,1008},{64,128},{80,16},{96,160},{112,4... | collective-permute-start | bytes 786440 | tf_op jit(solution)/shard_map/ppermute | solution.py:190
  70.7 5.4 %collective-permute-start.3 = (bf16[8,4096]{1,0:T(8,128)(2,1)}, bf16[8,4096]{1,0:T(8,128)(2,1)S(1)}, u32[]{:S(2)}, u32[]{:S(2)}) collective-permute-start(bf16[8,4096]{1,0:T(8,128)(2,1)} %slice.19), channel_id=1, source_target_pairs={{0,16},{16,32},{32,48},{48,64},{64,80},{80,96},{96,112},{112,128},... | collective-permute-start | bytes 196616 | tf_op jit(solution)/shard_map/ppermute | solution.py:213
  84.0 4.7 %collective-permute-start.4 = (bf16[1536,256]{1,0:T(8,128)(2,1)S(1)}, bf16[1536,256]{1,0:T(8,128)(2,1)S(1)}, u32[]{:S(2)}, u32[]{:S(2)}) collective-permute-start(bf16[1536,256]{1,0:T(8,128)(2,1)S(1)} %pad_maximum_fusion.near), channel_id=1, source_target_pairs={{0,16},{16,0},{32,48},{48,32},{64,80},{80,64},{96,112},{112,96},{1... | collective-permute-start | bytes 2359304 | tf_op jit(solution)/shard_map/ppermute | solution.py:194
  107.1 1.3 copy-start.1
  108.5 0.7 copy-start.4
  109.1 32.7 %all-to-all-start.1 = ((bf16[16,264,256]{2,1,0:T(8,128)(2,1)}), bf16[16,264,256]{2,1,0:T(8,128)(2,1)S(1)}, u32[]{:S(2)}, u32[]{:S(2)}) async-start(bf16[16,264,256]{2,1,0:T(8,128)(2,1)} %copy-done.1), calls=%async_computation.1 | async-start | bytes 4325376 | tf_op jit(solution)/shard_map/all_to_all | solution.py:252
  113.9 10.2 %collective-permute-start.5 = (bf16[1024,256]{1,0:T(8,128)(2,1)S(1)}, bf16[1024,256]{1,0:T(8,128)(2,1)S(1)}, u32[]{:S(2)}, u32[]{:S(2)}) collective-permute-start(bf16[1024,256]{1,0:T(8,128)(2,1)S(1)} %pad_maximum_fusion.2.own), channel_id=1, source_target_pairs={{0,32},{16,1008},{32,64},{48,16},{64,96},{80,48},{96,128},{112,80}... | collective-permute-start | bytes 1572872 | tf_op jit(solution)/shard_map/ppermute | solution.py:190
  115.8 13.5 %collective-permute-start.6 = (bf16[512,256]{1,0:T(8,128)(2,1)}, bf16[512,256]{1,0:T(8,128)(2,1)S(1)}, u32[]{:S(2)}, u32[]{:S(2)}) collective-permute-start(bf16[512,256]{1,0:T(8,128)(2,1)} %get-tuple-element.23), channel_id=1, source_target_pairs={{0,64},{16,976},{32,96},{48,1008},{64,128},{80,16},{96,160},{112,4... | collective-permute-start | bytes 786440 | tf_op jit(solution)/shard_map/ppermute | solution.py:190
  129.3 5.3 %collective-permute-start.7 = (bf16[1536,256]{1,0:T(8,128)(2,1)S(1)}, bf16[1536,256]{1,0:T(8,128)(2,1)S(1)}, u32[]{:S(2)}, u32[]{:S(2)}) collective-permute-start(bf16[1536,256]{1,0:T(8,128)(2,1)S(1)} %constant_dynamic-update-slice_fusion.near), channel_id=1, source_target_pairs={{0,16},{16,0},{32,48},{48,32},{64,80},{80,64},{96,112},{112,96},{1... | collective-permute-start | bytes 2359304 | tf_op jit(solution)/shard_map/ppermute | solution.py:194
  134.6 0.9 copy-start.2
  141.9 1.1 copy-start.3
  143.0 17.6 %copy-start.5 = (bf16[264,256]{1,0:T(8,128)(2,1)S(1)}, bf16[264,256]{1,0:T(8,128)(2,1)}, u32[]{:S(2)}) copy-start(bf16[264,256]{1,0:T(8,128)(2,1)} %copy-done.4) | copy-start | bytes 405508

commit v4 on v3

--- a/solution.py
+++ b/solution.py
@@ -128,20 +128,24 @@
     store_gated(gate(acc, taps[0]), out, True)
 
 
-def second_kernel(x, gain, taps, own, near, near_far, out, wb, w):
+def scale_kernel(x, out):
+    chunks, _, width = x.shape
+    squares = None
+    for k in range(chunks):
+        p = x[k].astype(F32)
+        s = jnp.sum(p * p, axis=1, keepdims=True)
+        squares = s if squares is None else squares + s
+    out[...] = lax.rsqrt(squares / (chunks * width) + EPS)
+
+
+def second_kernel(x, scale, gain, taps, own, near, near_far, out, wb, w):
     assemble((own, near, near_far), w)
     back_weights(w, wb)
     chunks, width = x.shape[0], x.shape[2]
-    squares = None
-    for k in range(chunks):
-        p = x[k].astype(F32)
-        s = jnp.sum(p * p, axis=1, keepdims=True)
-        squares = s if squares is None else squares + s
-    scale = lax.rsqrt(squares / (chunks * width) + EPS)
     acc = None
     for k in range(chunks):
         cols = slice(k * width, (k + 1) * width)
-        normed = (x[k].astype(F32) * scale * gain[1:2, cols]).astype(BF16)
+        normed = (x[k].astype(F32) * scale[...] * gain[1:2, cols]).astype(BF16)
         d = jnp.dot(normed, w[cols, :], preferred_element_type=F32)
         acc = d if acc is None else acc + d
     store_gated(gate(acc, taps[1]), out, False)
@@ -250,11 +254,14 @@
         3, [], 2 * rows * 1024 * 256, 4 << 20,
     )(whole, back, resid)
     current = send(spread)
+    scale = call(
+        scale_kernel, jax.ShapeDtypeStruct((rows, 1), F32), 1, [], 3 * rows * width, 2 << 20
+    )(current)
     gated, back = call(
         second_kernel,
         [jax.ShapeDtypeStruct((tp, count // 2, 128), BF16), back_shape],
-        6, [weights], flops, 8 << 20,
-    )(current, norm_gain, taps, *held[1])
+        7, [weights], flops, 8 << 20,
+    )(current, scale, norm_gain, taps, *held[1])
     whole = send(gated)
     (result,) = call(
         functools.partial(back_kernel, False),

time: 162 us -> 163 us (level)
  local copies, waits for them, and re-layouts: 5.5 us -> 3.49 us
    all_to_all x1, waiting for transfers between devices: 6.35 us -> 9.13 us  [per_device(): current = send(spread)]
    unnamed x18 -> x14, local copies, waits for them, and re-layouts: 4.07 us -> 2.06 us
    ppermute x3, waiting for transfers between devices: 4.53 us -> 2.65 us  [swap_cores(): return lax.ppermute(block, 'sp', [(i, i ^ 1) for i in range(64)])]
  transfers between devices with their start and end apart: 9 -> 9, of which waited for: 8 -> 7; matrix products, arithmetic and copies ran while one was open for 2% -> 2% of each run, Pallas kernels for 0% -> 0%
where the time goes in v4:
time: 163 us; the launch traced here: 162 us
  blocking collectives  85.4 us (52%)
  starting transfers between devices  34.4 us (21%)
  waiting for transfers between devices  28.5 us (17%)
  Pallas kernels  7.77 us (5%)
  local copies, waits for them, and re-layouts  3.49 us (2%)
  other arithmetic  2.13 us (1%)
    all_gather x1, blocking collectives, gather_far(): lax.all_gather(blocks, 'sp', axis=1, tiled=True, axis_index_groups=groups)  53 us
    all_to_all x2, blocking collectives, per_device(): whole = send(gated)  32.4 us
    ppermute x3, starting transfers between devices, swap_cores(): return lax.ppermute(block, 'sp', [(i, i ^ 1) for i in range(64)])  15.3 us
    ppermute x4, waiting for transfers between devices, exchange(): lax.ppermute(block, 'sp', [(i, (i + step[i % 2]) % 64) for i in range(64)])  14.6 us
    ppermute x4, starting transfers between devices, exchange(): lax.ppermute(block, 'sp', [(i, (i + step[i % 2]) % 64) for i in range(64)])  12.2 us
    all_to_all x1, waiting for transfers between devices, per_device(): current = send(spread)  9.13 us
    all_to_all x1, starting transfers between devices, per_device(): current = send(spread)  3.72 us
  transfers between devices with their start and end apart: 9, of which 7 were waited for; matrix products, arithmetic and copies ran while one was open for 2% of the time, Pallas kernels for 0%

profile of v4, /device:TPU:1, one launch (start us, length us, event | category | flops | bytes accessed | tf_op | source)
XLA Modules:
  0.0 161.9 jit_solution(1856232393454004338)
XLA Ops:
  0.0 1.7 %shard_map.73 = bf16[2,64,256]{2,1,0:T(8,128)(2,1)} custom-call(bf16[2,64,64]{2,1,0:T(8,128)(2,1)} %refs_0_.1, bf16[2,64,64]{2,1,0:T(8,128)(2,1)} %refs_1_.1, bf16[2,64,64]{2,1,0:T(8,128)(2,1)} %refs_2_.1, bf16[2,16,256]{2,1,0:T(8,128)(2,1)} %refs_3_.1), custom_call_target="tpu_custom_call" | custom-call | tf_op jit(solution)/shard_map/pallas_call | solution.py:41
  1.8 53.0 %all_gather.3 = bf16[2,512,256]{2,1,0:T(8,128)(2,1)S(1)} all-gather(bf16[2,64,256]{2,1,0:T(8,128)(2,1)} %shard_map.73), channel_id=1, replica_groups={{0,128,256,384,512,640,768,896},{16,144,272,400,528,656,784,912},{32,16..., dimensions={1}, use_global_device_ids=true | all-gather | bytes 589824 | tf_op jit(solution)/shard_map/all_gather | solution.py:203
  54.7 9.0 %collective-permute-start = (bf16[2,512,256]{2,1,0:T(8,128)(2,1)S(1)}, bf16[2,512,256]{2,1,0:T(8,128)(2,1)S(1)}, u32[]{:S(2)}, u32[]{:S(2)}) collective-permute-start(bf16[2,512,256]{2,1,0:T(8,128)(2,1)S(1)} %all_gather.3), channel_id=1, source_target_pairs={{0,16},{16,0},{32,48},{48,32},{64,80},{80,64},{96,112},{112,96},{1... | collective-permute-start | bytes 1572872 | tf_op jit(solution)/shard_map/ppermute | solution.py:198
  65.4 2.8 %collective-permute-start.1 = (bf16[1024,256]{1,0:T(8,128)(2,1)S(1)}, bf16[1024,256]{1,0:T(8,128)(2,1)}, u32[]{:S(2)}, u32[]{:S(2)}) collective-permute-start(bf16[1024,256]{1,0:T(8,128)(2,1)S(1)} %pad_maximum_fusion.1.own), channel_id=1, source_target_pairs={{0,32},{16,1008},{32,64},{48,16},{64,96},{80,48},{96,128},{112,80}... | collective-permute-start | bytes 1572872 | tf_op jit(solution)/shard_map/ppermute | solution.py:194
  68.2 1.9 %collective-permute-start.2 = (bf16[512,256]{1,0:T(8,128)(2,1)S(1)}, bf16[512,256]{1,0:T(8,128)(2,1)S(1)}, u32[]{:S(2)}, u32[]{:S(2)}) collective-permute-start(bf16[512,256]{1,0:T(8,128)(2,1)S(1)} %get-tuple-element.24), channel_id=1, source_target_pairs={{0,64},{16,976},{32,96},{48,1008},{64,128},{80,16},{96,160},{112,4... | collective-permute-start | bytes 786440 | tf_op jit(solution)/shard_map/ppermute | solution.py:194
  70.7 3.2 %collective-permute-start.3 = (bf16[8,4096]{1,0:T(8,128)(2,1)}, bf16[8,4096]{1,0:T(8,128)(2,1)S(1)}, u32[]{:S(2)}, u32[]{:S(2)}) collective-permute-start(bf16[8,4096]{1,0:T(8,128)(2,1)} %slice.19), channel_id=1, source_target_pairs={{0,16},{16,32},{32,48},{48,64},{64,80},{80,96},{96,112},{112,128},... | collective-permute-start | bytes 196616 | tf_op jit(solution)/shard_map/ppermute | solution.py:217
  74.0 2.2 %collective-permute-done.3.before = bf16[8,4096]{1,0:T(8,128)(2,1)S(1)} collective-permute-done((bf16[8,4096]{1,0:T(8,128)(2,1)}, bf16[8,4096]{1,0:T(8,128)(2,1)S(1)}, u32[]{:S(2)}, u32[]{:S(2)}) %collective-permute-start.3) | collective-permute-done | bytes 65568 | tf_op jit(solution)/shard_map/ppermute | solution.py:217
  76.2 6.7 %collective-permute-done.2 = bf16[512,256]{1,0:T(8,128)(2,1)S(1)} collective-permute-done((bf16[512,256]{1,0:T(8,128)(2,1)S(1)}, bf16[512,256]{1,0:T(8,128)(2,1)S(1)}, u32[]{:S(2)}, u32[]{:S(2)}) %collective-permute-start.2) | collective-permute-done | bytes 262176 | tf_op jit(solution)/shard_map/ppermute | solution.py:194
  82.9 1.1 pad_maximum_fusion.near
  84.0 2.8 %collective-permute-start.4 = (bf16[1536,256]{1,0:T(8,128)(2,1)S(1)}, bf16[1536,256]{1,0:T(8,128)(2,1)S(1)}, u32[]{:S(2)}, u32[]{:S(2)}) collective-permute-start(bf16[1536,256]{1,0:T(8,128)(2,1)S(1)} %pad_maximum_fusion.near), channel_id=1, source_target_pairs={{0,16},{16,0},{32,48},{48,32},{64,80},{80,64},{96,112},{112,96},{1... | collective-permute-start | bytes 2359304 | tf_op jit(solution)/shard_map/ppermute | solution.py:198
  86.8 1.9 %collective-permute-done.4.near_far = bf16[1536,256]{1,0:T(8,128)(2,1)S(1)} collective-permute-done((bf16[1536,256]{1,0:T(8,128)(2,1)S(1)}, bf16[1536,256]{1,0:T(8,128)(2,1)S(1)}, u32[]{:S(2)}, u32[]{:S(2)}) %collective-permute-start.4) | collective-permute-done | bytes 786464 | tf_op jit(solution)/shard_map/ppermute | solution.py:198
  88.7 1.6 shard_map.74
  90.3 16.4 %all_to_all.15.gathered = bf16[16,136,128]{2,1,0:T(8,128)(2,1)S(1)} all-to-all(bf16[16,136,128]{2,1,0:T(8,128)(2,1)S(1)} %get-tuple-element.16), channel_id=1, replica_groups=mesh['sp'=64,'tp'=16] {'tp'}, dimensions={0} | all-to-all | bytes 1114112 | tf_op jit(solution)/shard_map/all_to_all | solution.py:247
  107.1 1.3 copy-done.1
  109.1 3.7 %all-to-all-start.1 = ((bf16[16,264,256]{2,1,0:T(8,128)(2,1)}), bf16[16,264,256]{2,1,0:T(8,128)(2,1)S(1)}, u32[]{:S(2)}, u32[]{:S(2)}) async-start(bf16[16,264,256]{2,1,0:T(8,128)(2,1)} %copy-done.1), calls=%async_computation.1 | async-start | bytes 4325376 | tf_op jit(solution)/shard_map/all_to_all | solution.py:256
  113.9 1.9 %collective-permute-start.5 = (bf16[1024,256]{1,0:T(8,128)(2,1)S(1)}, bf16[1024,256]{1,0:T(8,128)(2,1)S(1)}, u32[]{:S(2)}, u32[]{:S(2)}) collective-permute-start(bf16[1024,256]{1,0:T(8,128)(2,1)S(1)} %pad_maximum_fusion.2.own), channel_id=1, source_target_pairs={{0,32},{16,1008},{32,64},{48,16},{64,96},{80,48},{96,128},{112,80}... | collective-permute-start | bytes 1572872 | tf_op jit(solution)/shard_map/ppermute | solution.py:194
  115.8 5.6 %collective-permute-start.6 = (bf16[512,256]{1,0:T(8,128)(2,1)}, bf16[512,256]{1,0:T(8,128)(2,1)S(1)}, u32[]{:S(2)}, u32[]{:S(2)}) collective-permute-start(bf16[512,256]{1,0:T(8,128)(2,1)} %get-tuple-element.23), channel_id=1, source_target_pairs={{0,64},{16,976},{32,96},{48,1008},{64,128},{80,16},{96,160},{112,4... | collective-permute-start | bytes 786440 | tf_op jit(solution)/shard_map/ppermute | solution.py:194
  121.4 2.7 %collective-permute-done.5 = bf16[1024,256]{1,0:T(8,128)(2,1)S(1)} collective-permute-done((bf16[1024,256]{1,0:T(8,128)(2,1)S(1)}, bf16[1024,256]{1,0:T(8,128)(2,1)S(1)}, u32[]{:S(2)}, u32[]{:S(2)}) %collective-permute-start.5) | collective-permute-done | bytes 524320 | tf_op jit(solution)/shard_map/ppermute | solution.py:194
  124.1 5.2 %collective-permute-done.6 = bf16[512,256]{1,0:T(8,128)(2,1)S(1)} collective-permute-done((bf16[512,256]{1,0:T(8,128)(2,1)}, bf16[512,256]{1,0:T(8,128)(2,1)S(1)}, u32[]{:S(2)}, u32[]{:S(2)}) %collective-permute-start.6) | collective-permute-done | bytes 262176 | tf_op jit(solution)/shard_map/ppermute | solution.py:194
  129.3 3.4 %collective-permute-start.7 = (bf16[1536,256]{1,0:T(8,128)(2,1)S(1)}, bf16[1536,256]{1,0:T(8,128)(2,1)}, u32[]{:S(2)}, u32[]{:S(2)}) collective-permute-start(bf16[1536,256]{1,0:T(8,128)(2,1)S(1)} %constant_dynamic-update-slice_fusion.near), channel_id=1, source_target_pairs={{0,16},{16,0},{32,48},{48,32},{64,80},{80,64},{96,112},{112,96},{1... | collective-permute-start | bytes 2359304 | tf_op jit(solution)/shard_map/ppermute | solution.py:198
  132.8 9.1 %all-to-all-done.1.x = bf16[16,264,256]{2,1,0:T(8,128)(2,1)S(1)} async-done(((bf16[16,264,256]{2,1,0:T(8,128)(2,1)}), bf16[16,264,256]{2,1,0:T(8,128)(2,1)S(1)}, u32[]{:S(2)}, u32[]{:S(2)}) %all-to-all-start.1) | async-done | bytes 2162720 | tf_op jit(solution)/shard_map/all_to_all | solution.py:256
  142.6 2.3 %shard_map.77 = (bf16[16,128,128]{2,1,0:T(8,128)(2,1)S(1)}, bf16[1024,256]{1,0:T(8,128)(2,1)S(1)}) custom-call(bf16[16,264,256]{2,1,0:T(8,128)(2,1)S(1)} %all-to-all-done.1.x, f32[264,1]{1,0:T(8,128)S(1)} %shard_map.76.scale, f32[2,4096]{1,0:T(2,128)S(1)} %copy-done.4, f32[2,3,64]{2,1,0:T(4,128)S(1)} %copy.8.taps, ...), custom_call_target="tpu_custom_call" | custom-call | flops 553648128 | bytes 8388608 | tf_op jit(solution)/shard_map/pallas_call | solution.py:260
  144.9 16.0 %all_to_all.16.gathered = bf16[16,128,128]{2,1,0:T(8,128)(2,1)S(1)} all-to-all(bf16[16,128,128]{2,1,0:T(8,128)(2,1)S(1)} %get-tuple-element.20), channel_id=1, replica_groups=mesh['sp'=64,'tp'=16] {'tp'}, dimensions={0} | all-to-all | bytes 1048576 | tf_op jit(solution)/shard_map/all_to_all | solution.py:265
  160.9 1.0 shard_map.78
  (25 shorter events, 5.1 us)
Async XLA Ops:
  0.0 70.1 %copy-start = (bf16[256,4096]{1,0:T(8,128)(2,1)S(1)}, bf16[256,4096]{1,0:T(8,128)(2,1)}, u32[]{:S(2)}) copy-start(bf16[256,4096]{1,0:T(8,128)(2,1)} %x.1) | copy-start | bytes 6291460
  54.7 10.6 %collective-permute-start = (bf16[2,512,256]{2,1,0:T(8,128)(2,1)S(1)}, bf16[2,512,256]{2,1,0:T(8,128)(2,1)S(1)}, u32[]{:S(2)}, u32[]{:S(2)}) collective-permute-start(bf16[2,512,256]{2,1,0:T(8,128)(2,1)S(1)} %all_gather.3), channel_id=1, source_target_pairs={{0,16},{16,0},{32,48},{48,32},{64,80},{80,64},{96,112},{112,96},{1... | collective-permute-start | bytes 1572872 | tf_op jit(solution)/shard_map/ppermute | solution.py:198
  65.4 21.4 %copy-start.5 = (f32[2,3,64]{2,0,1:T(2,128)S(1)}, f32[2,3,64]{2,0,1:T(2,128)}, u32[]{:S(2)}) copy-start(f32[2,3,64]{2,0,1:T(2,128)} %param.13) | copy-start | bytes 4612
  65.4 23.3 %copy-start.4 = (f32[2,4096]{1,0:T(2,128)S(1)}, f32[2,4096]{1,0:T(2,128)}, u32[]{:S(2)}) copy-start(f32[2,4096]{1,0:T(2,128)} %gain.3) | copy-start | bytes 98308
  65.4 17.5 %collective-permute-start.1 = (bf16[1024,256]{1,0:T(8,128)(2,1)S(1)}, bf16[1024,256]{1,0:T(8,128)(2,1)}, u32[]{:S(2)}, u32[]{:S(2)}) collective-permute-start(bf16[1024,256]{1,0:T(8,128)(2,1)S(1)} %pad_maximum_fusion.1.own), channel_id=1, source_target_pairs={{0,32},{16,1008},{32,64},{48,16},{64,96},{80,48},{96,128},{112,80}... | collective-permute-start | bytes 1572872 | tf_op jit(solution)/shard_map/ppermute | solution.py:194
  68.2 14.7 %collective-permute-start.2 = (bf16[512,256]{1,0:T(8,128)(2,1)S(1)}, bf16[512,256]{1,0:T(8,128)(2,1)S(1)}, u32[]{:S(2)}, u32[]{:S(2)}) collective-permute-start(bf16[512,256]{1,0:T(8,128)(2,1)S(1)} %get-tuple-element.24), channel_id=1, source_target_pairs={{0,64},{16,976},{32,96},{48,1008},{64,128},{80,16},{96,160},{112,4... | collective-permute-start | bytes 786440 | tf_op jit(solution)/shard_map/ppermute | solution.py:194
  70.7 5.4 %collective-permute-start.3 = (bf16[8,4096]{1,0:T(8,128)(2,1)}, bf16[8,4096]{1,0:T(8,128)(2,1)S(1)}, u32[]{:S(2)}, u32[]{:S(2)}) collective-permute-start(bf16[8,4096]{1,0:T(8,128)(2,1)} %slice.19), channel_id=1, source_target_pairs={{0,16},{16,32},{32,48},{48,64},{64,80},{80,96},{96,112},{112,128},... | collective-permute-start | bytes 196616 | tf_op jit(solution)/shard_map/ppermute | solution.py:217
  84.0 4.7 %collective-permute-start.4 = (bf16[1536,256]{1,0:T(8,128)(2,1)S(1)}, bf16[1536,256]{1,0:T(8,128)(2,1)S(1)}, u32[]{:S(2)}, u32[]{:S(2)}) collective-permute-start(bf16[1536,256]{1,0:T(8,128)(2,1)S(1)} %pad_maximum_fusion.near), channel_id=1, source_target_pairs={{0,16},{16,0},{32,48},{48,32},{64,80},{80,64},{96,112},{112,96},{1... | collective-permute-start | bytes 2359304 | tf_op jit(solution)/shard_map/ppermute | solution.py:198
  107.1 1.4 copy-start.1
  108.5 0.7 copy-start.2
  109.1 32.7 %all-to-all-start.1 = ((bf16[16,264,256]{2,1,0:T(8,128)(2,1)}), bf16[16,264,256]{2,1,0:T(8,128)(2,1)S(1)}, u32[]{:S(2)}, u32[]{:S(2)}) async-start(bf16[16,264,256]{2,1,0:T(8,128)(2,1)} %copy-done.1), calls=%async_computation.1 | async-start | bytes 4325376 | tf_op jit(solution)/shard_map/all_to_all | solution.py:256
  113.9 10.2 %collective-permute-start.5 = (bf16[1024,256]{1,0:T(8,128)(2,1)S(1)}, bf16[1024,256]{1,0:T(8,128)(2,1)S(1)}, u32[]{:S(2)}, u32[]{:S(2)}) collective-permute-start(bf16[1024,256]{1,0:T(8,128)(2,1)S(1)} %pad_maximum_fusion.2.own), channel_id=1, source_target_pairs={{0,32},{16,1008},{32,64},{48,16},{64,96},{80,48},{96,128},{112,80}... | collective-permute-start | bytes 1572872 | tf_op jit(solution)/shard_map/ppermute | solution.py:194
  115.8 13.5 %collective-permute-start.6 = (bf16[512,256]{1,0:T(8,128)(2,1)}, bf16[512,256]{1,0:T(8,128)(2,1)S(1)}, u32[]{:S(2)}, u32[]{:S(2)}) collective-permute-start(bf16[512,256]{1,0:T(8,128)(2,1)} %get-tuple-element.23), channel_id=1, source_target_pairs={{0,64},{16,976},{32,96},{48,1008},{64,128},{80,16},{96,160},{112,4... | collective-permute-start | bytes 786440 | tf_op jit(solution)/shard_map/ppermute | solution.py:194
  129.3 13.2 %collective-permute-start.7 = (bf16[1536,256]{1,0:T(8,128)(2,1)S(1)}, bf16[1536,256]{1,0:T(8,128)(2,1)}, u32[]{:S(2)}, u32[]{:S(2)}) collective-permute-start(bf16[1536,256]{1,0:T(8,128)(2,1)S(1)} %constant_dynamic-update-slice_fusion.near), channel_id=1, source_target_pairs={{0,16},{16,0},{32,48},{48,32},{64,80},{80,64},{96,112},{112,96},{1... | collective-permute-start | bytes 2359304 | tf_op jit(solution)/shard_map/ppermute | solution.py:198
  142.5 18.4 %copy-start.3 = (bf16[264,256]{1,0:T(8,128)(2,1)S(1)}, bf16[264,256]{1,0:T(8,128)(2,1)}, u32[]{:S(2)}) copy-start(bf16[264,256]{1,0:T(8,128)(2,1)} %copy-done.2) | copy-start | bytes 405508

commit v5 on v3

--- a/solution.py
+++ b/solution.py
@@ -128,7 +128,8 @@
     store_gated(gate(acc, taps[0]), out, True)
 
 
-def second_kernel(x, gain, taps, own, near, near_far, out, wb, w):
+def second_kernel(x, gain, taps, own, near, near_far, out, wb, resid, w):
+    resid[...] = x[lax.axis_index("tp")]
     assemble((own, near, near_far), w)
     back_weights(w, wb)
     chunks, width = x.shape[0], x.shape[2]
@@ -166,9 +167,8 @@
     start = resid.shape[0] - proj.shape[0]
     new = (resid[...].astype(F32)[start:] + proj).astype(BF16)
     if halo:
-        outs[0][...] = new
         for j in range(count):
-            outs[1][j, :, :] = new
+            outs[0][j, :, :] = new
     else:
         outs[0][...] = new
 
@@ -196,9 +196,13 @@
 
 def gather_far(blocks):
     groups = [[r + 8 * k for k in range(8)] for r in range(8)]
-    return lax.all_gather(
-        blocks, "sp", axis=1, tiled=True, axis_index_groups=groups
-    )
+    flat = blocks.reshape(-1, blocks.shape[2])
+    return lax.all_gather(flat, "sp", axis=0, tiled=True, axis_index_groups=groups)
+
+
+def layer_of(far, layer):
+    parts = far.reshape(8, -1, ROWS, far.shape[1])
+    return parts[:, layer].reshape(-1, far.shape[1])
 
 
 def per_device(tokens, norm_gain, w_outer, w_inner, w_value, w_back, taps):
@@ -214,11 +218,11 @@
     far = gather_far(packed)
     twos = []
     for layer in range(layers):
-        twos.append(exchange(far[layer], 2))
+        twos.append(exchange(layer_of(far, layer), 2))
     partner = swap_cores(far)
     held = []
     for layer in range(layers):
-        both = jnp.concatenate([far[layer], partner[layer]], axis=0)
+        both = jnp.concatenate([layer_of(far, layer), layer_of(partner, layer)], axis=0)
         one = exchange(both, 1)
         near = jnp.concatenate([one, twos[layer]], axis=0)
         if layer == 0:
@@ -241,18 +245,19 @@
         7, [weights], flops, 8 << 20,
     )(tokens, before, norm_gain, taps, *held[0])
     whole = send(gated)
-    resid, spread = call(
+    (spread,) = call(
         functools.partial(back_kernel, True),
-        [
-            jax.ShapeDtypeStruct((rows, feats), BF16),
-            jax.ShapeDtypeStruct((tp, rows, feats), BF16),
-        ],
+        [jax.ShapeDtypeStruct((tp, rows, feats), BF16)],
         3, [], 2 * rows * 1024 * 256, 4 << 20,
     )(whole, back, resid)
     current = send(spread)
-    gated, back = call(
+    gated, back, resid = call(
         second_kernel,
-        [jax.ShapeDtypeStruct((tp, count // 2, 128), BF16), back_shape],
+        [
+            jax.ShapeDtypeStruct((tp, count // 2, 128), BF16),
+            back_shape,
+            jax.ShapeDtypeStruct((rows, feats), BF16),
+        ],
         6, [weights], flops, 8 << 20,
     )(current, norm_gain, taps, *held[1])
     whole = send(gated)

time: 162 us -> 162 us (level)
    unnamed x18 -> x14, local copies, waits for them, and re-layouts: 4.07 us -> 3.41 us
where the time goes in v5:
time: 162 us; the launch traced here: 161 us
  blocking collectives  85.4 us (53%)
  starting transfers between devices  34.4 us (21%)
  waiting for transfers between devices  27.6 us (17%)
  Pallas kernels  6.41 us (4%)
  local copies, waits for them, and re-layouts  4.84 us (3%)
  other arithmetic  2.13 us (1%)
    all_gather x1, blocking collectives, gather_far(): lax.all_gather(flat, 'sp', axis=0, tiled=True, axis_index_groups=groups)  53 us
    all_to_all x2, blocking collectives, per_device(): whole = send(gated)  32.4 us
    ppermute x3, starting transfers between devices, swap_cores(): return lax.ppermute(block, 'sp', [(i, i ^ 1) for i in range(64)])  15.3 us
    ppermute x4, waiting for transfers between devices, exchange(): lax.ppermute(block, 'sp', [(i, (i + step[i % 2]) % 64) for i in range(64)])  14.6 us
    ppermute x4, starting transfers between devices, exchange(): lax.ppermute(block, 'sp', [(i, (i + step[i % 2]) % 64) for i in range(64)])  12.2 us
    all_to_all x1, waiting for transfers between devices, per_device(): current = send(spread)  6.35 us
    ppermute x3, waiting for transfers between devices, swap_cores(): return lax.ppermute(block, 'sp', [(i, i ^ 1) for i in range(64)])  4.53 us
    all_to_all x1, starting transfers between devices, per_device(): current = send(spread)  3.72 us
  transfers between devices with their start and end apart: 9, of which 8 were waited for; matrix products, arithmetic and copies ran while one was open for 2% of the time, Pallas kernels for 0%

profile of v5, /device:TPU:1, one launch (start us, length us, event | category | flops | bytes accessed | tf_op | source)
XLA Modules:
  0.0 161.0 jit_solution(16231774098471122504)
XLA Ops:
  0.0 1.7 %shard_map.73 = bf16[2,64,256]{2,1,0:T(8,128)(2,1)} custom-call(bf16[2,64,64]{2,1,0:T(8,128)(2,1)} %refs_0_.1, bf16[2,64,64]{2,1,0:T(8,128)(2,1)} %refs_1_.1, bf16[2,64,64]{2,1,0:T(8,128)(2,1)} %refs_2_.1, bf16[2,16,256]{2,1,0:T(8,128)(2,1)} %refs_3_.1), custom_call_target="tpu_custom_call" | custom-call | tf_op jit(solution)/shard_map/pallas_call | solution.py:41
  1.8 53.0 %all_gather.3 = bf16[1024,256]{1,0:T(8,128)(2,1)S(1)} all-gather(bf16[128,256]{1,0:T(8,128)(2,1)} %bitcast.13), channel_id=1, replica_groups={{0,128,256,384,512,640,768,896},{16,144,272,400,528,656,784,912},{32,16..., dimensions={0}, use_global_device_ids=true | all-gather | bytes 589824 | tf_op jit(solution)/shard_map/all_gather | solution.py:200
  54.7 9.0 %collective-permute-start = (bf16[1024,256]{1,0:T(8,128)(2,1)S(1)}, bf16[1024,256]{1,0:T(8,128)(2,1)S(1)}, u32[]{:S(2)}, u32[]{:S(2)}) collective-permute-start(bf16[1024,256]{1,0:T(8,128)(2,1)S(1)} %all_gather.3), channel_id=1, source_target_pairs={{0,16},{16,0},{32,48},{48,32},{64,80},{80,64},{96,112},{112,96},{1... | collective-permute-start | bytes 1572872 | tf_op jit(solution)/shard_map/ppermute | solution.py:194
  65.4 2.8 %collective-permute-start.1 = (bf16[1024,256]{1,0:T(8,128)(2,1)S(1)}, bf16[1024,256]{1,0:T(8,128)(2,1)}, u32[]{:S(2)}, u32[]{:S(2)}) collective-permute-start(bf16[1024,256]{1,0:T(8,128)(2,1)S(1)} %pad_maximum_fusion.1.own), channel_id=1, source_target_pairs={{0,32},{16,1008},{32,64},{48,16},{64,96},{80,48},{96,128},{112,80}... | collective-permute-start | bytes 1572872 | tf_op jit(solution)/shard_map/ppermute | solution.py:190
  68.2 1.9 %collective-permute-start.2 = (bf16[512,256]{1,0:T(8,128)(2,1)S(1)}, bf16[512,256]{1,0:T(8,128)(2,1)S(1)}, u32[]{:S(2)}, u32[]{:S(2)}) collective-permute-start(bf16[512,256]{1,0:T(8,128)(2,1)S(1)} %bitcast.10), channel_id=1, source_target_pairs={{0,64},{16,976},{32,96},{48,1008},{64,128},{80,16},{96,160},{112,4... | collective-permute-start | bytes 786440 | tf_op jit(solution)/shard_map/ppermute | solution.py:190
  70.7 3.2 %collective-permute-start.3 = (bf16[8,4096]{1,0:T(8,128)(2,1)}, bf16[8,4096]{1,0:T(8,128)(2,1)S(1)}, u32[]{:S(2)}, u32[]{:S(2)}) collective-permute-start(bf16[8,4096]{1,0:T(8,128)(2,1)} %slice.19), channel_id=1, source_target_pairs={{0,16},{16,32},{32,48},{48,64},{64,80},{80,96},{96,112},{112,128},... | collective-permute-start | bytes 196616 | tf_op jit(solution)/shard_map/ppermute | solution.py:217
  74.0 2.2 %collective-permute-done.3.before = bf16[8,4096]{1,0:T(8,128)(2,1)S(1)} collective-permute-done((bf16[8,4096]{1,0:T(8,128)(2,1)}, bf16[8,4096]{1,0:T(8,128)(2,1)S(1)}, u32[]{:S(2)}, u32[]{:S(2)}) %collective-permute-start.3) | collective-permute-done | bytes 65568 | tf_op jit(solution)/shard_map/ppermute | solution.py:217
  76.2 6.7 %collective-permute-done.2 = bf16[512,256]{1,0:T(8,128)(2,1)S(1)} collective-permute-done((bf16[512,256]{1,0:T(8,128)(2,1)S(1)}, bf16[512,256]{1,0:T(8,128)(2,1)S(1)}, u32[]{:S(2)}, u32[]{:S(2)}) %collective-permute-start.2) | collective-permute-done | bytes 262176 | tf_op jit(solution)/shard_map/ppermute | solution.py:190
  84.0 2.8 %collective-permute-start.4 = (bf16[1536,256]{1,0:T(8,128)(2,1)S(1)}, bf16[1536,256]{1,0:T(8,128)(2,1)S(1)}, u32[]{:S(2)}, u32[]{:S(2)}) collective-permute-start(bf16[1536,256]{1,0:T(8,128)(2,1)S(1)} %pad_maximum_fusion.near), channel_id=1, source_target_pairs={{0,16},{16,0},{32,48},{48,32},{64,80},{80,64},{96,112},{112,96},{1... | collective-permute-start | bytes 2359304 | tf_op jit(solution)/shard_map/ppermute | solution.py:194
  86.8 1.9 %collective-permute-done.4.near_far = bf16[1536,256]{1,0:T(8,128)(2,1)S(1)} collective-permute-done((bf16[1536,256]{1,0:T(8,128)(2,1)S(1)}, bf16[1536,256]{1,0:T(8,128)(2,1)S(1)}, u32[]{:S(2)}, u32[]{:S(2)}) %collective-permute-start.4) | collective-permute-done | bytes 786464 | tf_op jit(solution)/shard_map/ppermute | solution.py:194
  88.7 1.6 shard_map.74
  90.3 16.4 %all_to_all.15.gathered = bf16[16,136,128]{2,1,0:T(8,128)(2,1)S(1)} all-to-all(bf16[16,136,128]{2,1,0:T(8,128)(2,1)S(1)} %get-tuple-element.15), channel_id=1, replica_groups=mesh['sp'=64,'tp'=16] {'tp'}, dimensions={0} | all-to-all | bytes 1114112 | tf_op jit(solution)/shard_map/all_to_all | solution.py:247
  107.1 1.3 copy-done.1
  108.5 3.7 %all-to-all-start.1 = ((bf16[16,264,256]{2,1,0:T(8,128)(2,1)}), bf16[16,264,256]{2,1,0:T(8,128)(2,1)S(1)}, u32[]{:S(2)}, u32[]{:S(2)}) async-start(bf16[16,264,256]{2,1,0:T(8,128)(2,1)} %copy-done.1), calls=%async_computation.1 | async-start | bytes 4325376 | tf_op jit(solution)/shard_map/all_to_all | solution.py:253
  113.2 1.9 %collective-permute-start.5 = (bf16[1024,256]{1,0:T(8,128)(2,1)S(1)}, bf16[1024,256]{1,0:T(8,128)(2,1)S(1)}, u32[]{:S(2)}, u32[]{:S(2)}) collective-permute-start(bf16[1024,256]{1,0:T(8,128)(2,1)S(1)} %pad_maximum_fusion.2.own), channel_id=1, source_target_pairs={{0,32},{16,1008},{32,64},{48,16},{64,96},{80,48},{96,128},{112,80}... | collective-permute-start | bytes 1572872 | tf_op jit(solution)/shard_map/ppermute | solution.py:190
  115.1 5.6 %collective-permute-start.6 = (bf16[512,256]{1,0:T(8,128)(2,1)}, bf16[512,256]{1,0:T(8,128)(2,1)S(1)}, u32[]{:S(2)}, u32[]{:S(2)}) collective-permute-start(bf16[512,256]{1,0:T(8,128)(2,1)} %bitcast.5), channel_id=1, source_target_pairs={{0,64},{16,976},{32,96},{48,1008},{64,128},{80,16},{96,160},{112,4... | collective-permute-start | bytes 786440 | tf_op jit(solution)/shard_map/ppermute | solution.py:190
  120.7 2.7 %collective-permute-done.5 = bf16[1024,256]{1,0:T(8,128)(2,1)S(1)} collective-permute-done((bf16[1024,256]{1,0:T(8,128)(2,1)S(1)}, bf16[1024,256]{1,0:T(8,128)(2,1)S(1)}, u32[]{:S(2)}, u32[]{:S(2)}) %collective-permute-start.5) | collective-permute-done | bytes 524320 | tf_op jit(solution)/shard_map/ppermute | solution.py:190
  123.5 5.2 %collective-permute-done.6 = bf16[512,256]{1,0:T(8,128)(2,1)S(1)} collective-permute-done((bf16[512,256]{1,0:T(8,128)(2,1)}, bf16[512,256]{1,0:T(8,128)(2,1)S(1)}, u32[]{:S(2)}, u32[]{:S(2)}) %collective-permute-start.6) | collective-permute-done | bytes 262176 | tf_op jit(solution)/shard_map/ppermute | solution.py:190
  128.7 3.4 %collective-permute-start.7 = (bf16[1536,256]{1,0:T(8,128)(2,1)S(1)}, bf16[1536,256]{1,0:T(8,128)(2,1)S(1)}, u32[]{:S(2)}, u32[]{:S(2)}) collective-permute-start(bf16[1536,256]{1,0:T(8,128)(2,1)S(1)} %constant_dynamic-update-slice_fusion.near), channel_id=1, source_target_pairs={{0,16},{16,0},{32,48},{48,32},{64,80},{80,64},{96,112},{112,96},{1... | collective-permute-start | bytes 2359304 | tf_op jit(solution)/shard_map/ppermute | solution.py:194
  132.1 1.9 %collective-permute-done.7.near_far = bf16[1536,256]{1,0:T(8,128)(2,1)S(1)} collective-permute-done((bf16[1536,256]{1,0:T(8,128)(2,1)S(1)}, bf16[1536,256]{1,0:T(8,128)(2,1)S(1)}, u32[]{:S(2)}, u32[]{:S(2)}) %collective-permute-start.7) | collective-permute-done | bytes 786464 | tf_op jit(solution)/shard_map/ppermute | solution.py:194
  134.9 6.4 %all-to-all-done.1.x = bf16[16,264,256]{2,1,0:T(8,128)(2,1)S(1)} async-done(((bf16[16,264,256]{2,1,0:T(8,128)(2,1)}), bf16[16,264,256]{2,1,0:T(8,128)(2,1)S(1)}, u32[]{:S(2)}, u32[]{:S(2)}) %all-to-all-start.1) | async-done | bytes 2162720 | tf_op jit(solution)/shard_map/all_to_all | solution.py:253
  141.2 1.1 copy-done.3
  142.4 1.6 shard_map.76
  144.0 16.0 %all_to_all.16.gathered = bf16[16,128,128]{2,1,0:T(8,128)(2,1)S(1)} all-to-all(bf16[16,128,128]{2,1,0:T(8,128)(2,1)S(1)} %get-tuple-element.18), channel_id=1, replica_groups=mesh['sp'=64,'tp'=16] {'tp'}, dimensions={0} | all-to-all | bytes 1048576 | tf_op jit(solution)/shard_map/all_to_all | solution.py:263
  (24 shorter events, 6.7 us)
Async XLA Ops:
  0.0 70.1 %copy-start = (bf16[256,4096]{1,0:T(8,128)(2,1)S(1)}, bf16[256,4096]{1,0:T(8,128)(2,1)}, u32[]{:S(2)}) copy-start(bf16[256,4096]{1,0:T(8,128)(2,1)} %x.1) | copy-start | bytes 6291460
  54.7 10.6 %collective-permute-start = (bf16[1024,256]{1,0:T(8,128)(2,1)S(1)}, bf16[1024,256]{1,0:T(8,128)(2,1)S(1)}, u32[]{:S(2)}, u32[]{:S(2)}) collective-permute-start(bf16[1024,256]{1,0:T(8,128)(2,1)S(1)} %all_gather.3), channel_id=1, source_target_pairs={{0,16},{16,0},{32,48},{48,32},{64,80},{80,64},{96,112},{112,96},{1... | collective-permute-start | bytes 1572872 | tf_op jit(solution)/shard_map/ppermute | solution.py:194
  65.4 21.4 %copy-start.5 = (f32[2,3,64]{2,0,1:T(2,128)S(1)}, f32[2,3,64]{2,0,1:T(2,128)}, u32[]{:S(2)}) copy-start(f32[2,3,64]{2,0,1:T(2,128)} %param.13) | copy-start | bytes 4612
  65.4 23.3 %copy-start.4 = (f32[2,4096]{1,0:T(2,128)S(1)}, f32[2,4096]{1,0:T(2,128)}, u32[]{:S(2)}) copy-start(f32[2,4096]{1,0:T(2,128)} %gain.3) | copy-start | bytes 98308
  65.4 17.5 %collective-permute-start.1 = (bf16[1024,256]{1,0:T(8,128)(2,1)S(1)}, bf16[1024,256]{1,0:T(8,128)(2,1)}, u32[]{:S(2)}, u32[]{:S(2)}) collective-permute-start(bf16[1024,256]{1,0:T(8,128)(2,1)S(1)} %pad_maximum_fusion.1.own), channel_id=1, source_target_pairs={{0,32},{16,1008},{32,64},{48,16},{64,96},{80,48},{96,128},{112,80}... | collective-permute-start | bytes 1572872 | tf_op jit(solution)/shard_map/ppermute | solution.py:190
  68.2 14.7 %collective-permute-start.2 = (bf16[512,256]{1,0:T(8,128)(2,1)S(1)}, bf16[512,256]{1,0:T(8,128)(2,1)S(1)}, u32[]{:S(2)}, u32[]{:S(2)}) collective-permute-start(bf16[512,256]{1,0:T(8,128)(2,1)S(1)} %bitcast.10), channel_id=1, source_target_pairs={{0,64},{16,976},{32,96},{48,1008},{64,128},{80,16},{96,160},{112,4... | collective-permute-start | bytes 786440 | tf_op jit(solution)/shard_map/ppermute | solution.py:190
  70.7 5.4 %collective-permute-start.3 = (bf16[8,4096]{1,0:T(8,128)(2,1)}, bf16[8,4096]{1,0:T(8,128)(2,1)S(1)}, u32[]{:S(2)}, u32[]{:S(2)}) collective-permute-start(bf16[8,4096]{1,0:T(8,128)(2,1)} %slice.19), channel_id=1, source_target_pairs={{0,16},{16,32},{32,48},{48,64},{64,80},{80,96},{96,112},{112,128},... | collective-permute-start | bytes 196616 | tf_op jit(solution)/shard_map/ppermute | solution.py:217
  84.0 4.7 %collective-permute-start.4 = (bf16[1536,256]{1,0:T(8,128)(2,1)S(1)}, bf16[1536,256]{1,0:T(8,128)(2,1)S(1)}, u32[]{:S(2)}, u32[]{:S(2)}) collective-permute-start(bf16[1536,256]{1,0:T(8,128)(2,1)S(1)} %pad_maximum_fusion.near), channel_id=1, source_target_pairs={{0,16},{16,0},{32,48},{48,32},{64,80},{80,64},{96,112},{112,96},{1... | collective-permute-start | bytes 2359304 | tf_op jit(solution)/shard_map/ppermute | solution.py:194
  107.1 1.3 copy-start.1
  108.5 32.7 %all-to-all-start.1 = ((bf16[16,264,256]{2,1,0:T(8,128)(2,1)}), bf16[16,264,256]{2,1,0:T(8,128)(2,1)S(1)}, u32[]{:S(2)}, u32[]{:S(2)}) async-start(bf16[16,264,256]{2,1,0:T(8,128)(2,1)} %copy-done.1), calls=%async_computation.1 | async-start | bytes 4325376 | tf_op jit(solution)/shard_map/all_to_all | solution.py:253
  113.2 10.2 %collective-permute-start.5 = (bf16[1024,256]{1,0:T(8,128)(2,1)S(1)}, bf16[1024,256]{1,0:T(8,128)(2,1)S(1)}, u32[]{:S(2)}, u32[]{:S(2)}) collective-permute-start(bf16[1024,256]{1,0:T(8,128)(2,1)S(1)} %pad_maximum_fusion.2.own), channel_id=1, source_target_pairs={{0,32},{16,1008},{32,64},{48,16},{64,96},{80,48},{96,128},{112,80}... | collective-permute-start | bytes 1572872 | tf_op jit(solution)/shard_map/ppermute | solution.py:190
  115.1 13.5 %collective-permute-start.6 = (bf16[512,256]{1,0:T(8,128)(2,1)}, bf16[512,256]{1,0:T(8,128)(2,1)S(1)}, u32[]{:S(2)}, u32[]{:S(2)}) collective-permute-start(bf16[512,256]{1,0:T(8,128)(2,1)} %bitcast.5), channel_id=1, source_target_pairs={{0,64},{16,976},{32,96},{48,1008},{64,128},{80,16},{96,160},{112,4... | collective-permute-start | bytes 786440 | tf_op jit(solution)/shard_map/ppermute | solution.py:190
  128.7 5.3 %collective-permute-start.7 = (bf16[1536,256]{1,0:T(8,128)(2,1)S(1)}, bf16[1536,256]{1,0:T(8,128)(2,1)S(1)}, u32[]{:S(2)}, u32[]{:S(2)}) collective-permute-start(bf16[1536,256]{1,0:T(8,128)(2,1)S(1)} %constant_dynamic-update-slice_fusion.near), channel_id=1, source_target_pairs={{0,16},{16,0},{32,48},{48,32},{64,80},{80,64},{96,112},{112,96},{1... | collective-permute-start | bytes 2359304 | tf_op jit(solution)/shard_map/ppermute | solution.py:194
  134.0 0.9 copy-start.2
  141.2 1.1 copy-start.3

commit v6 on v5

--- a/solution.py
+++ b/solution.py
@@ -167,8 +167,15 @@
     start = resid.shape[0] - proj.shape[0]
     new = (resid[...].astype(F32)[start:] + proj).astype(BF16)
     if halo:
-        for j in range(count):
-            outs[0][j, :, :] = new
+        spread, block, sems = outs
+        block[...] = new
+        copies = [
+            pltpu.make_async_copy(block, spread.at[j], sems.at[j]) for j in range(count)
+        ]
+        for copy in copies:
+            copy.start()
+        for copy in copies:
+            copy.wait()
     else:
         outs[0][...] = new
 
@@ -245,10 +252,19 @@
         7, [weights], flops, 8 << 20,
     )(tokens, before, norm_gain, taps, *held[0])
     whole = send(gated)
-    (spread,) = call(
+    spread = pl.pallas_call(
         functools.partial(back_kernel, True),
-        [jax.ShapeDtypeStruct((tp, rows, feats), BF16)],
-        3, [], 2 * rows * 1024 * 256, 4 << 20,
+        out_shape=jax.ShapeDtypeStruct((tp, rows, feats), BF16),
+        in_specs=[VMEM] * 3,
+        out_specs=pl.BlockSpec(memory_space=pltpu.HBM),
+        scratch_shapes=[
+            pltpu.VMEM((rows, feats), BF16),
+            pltpu.SemaphoreType.DMA((tp,)),
+        ],
+        compiler_params=pltpu.CompilerParams(vmem_limit_bytes=62 << 20),
+        cost_estimate=pl.CostEstimate(
+            flops=2 * rows * 1024 * 256, bytes_accessed=4 << 20, transcendentals=0
+        ),
     )(whole, back, resid)
     current = send(spread)
     gated, back, resid = call(

time: 162 us -> 163 us (level)
  Pallas kernels: 6.41 us -> 9.05 us
    pallas_call x1, Pallas kernels: 0.45 us -> 3.08 us  [per_device(): pl.pallas_call(functools.partial(back_kernel, True), out_shape=jax.ShapeD...]
where the time goes in v6:
time: 163 us; the launch traced here: 162 us
  blocking collectives  85.5 us (52%)
  starting transfers between devices  34.4 us (21%)
  waiting for transfers between devices  27 us (17%)
  Pallas kernels  9.05 us (6%)
  local copies, waits for them, and re-layouts  3.5 us (2%)
  other arithmetic  2.79 us (2%)
    all_gather x1, blocking collectives, gather_far(): lax.all_gather(flat, 'sp', axis=0, tiled=True, axis_index_groups=groups)  53 us
    all_to_all x2, blocking collectives, per_device(): whole = send(gated)  32.5 us
    ppermute x3, starting transfers between devices, swap_cores(): return lax.ppermute(block, 'sp', [(i, i ^ 1) for i in range(64)])  15.3 us
    ppermute x4, waiting for transfers between devices, exchange(): lax.ppermute(block, 'sp', [(i, (i + step[i % 2]) % 64) for i in range(64)])  13.9 us
    ppermute x4, starting transfers between devices, exchange(): lax.ppermute(block, 'sp', [(i, (i + step[i % 2]) % 64) for i in range(64)])  12.2 us
    all_to_all x1, waiting for transfers between devices, per_device(): current = send(spread)  6.35 us
    ppermute x3, waiting for transfers between devices, swap_cores(): return lax.ppermute(block, 'sp', [(i, i ^ 1) for i in range(64)])  4.54 us
    all_to_all x1, starting transfers between devices, per_device(): current = send(spread)  3.73 us
  transfers between devices with their start and end apart: 9, of which 8 were waited for; matrix products, arithmetic and copies ran while one was open for 2% of the time, Pallas kernels for 0%

profile of v6, /device:TPU:1, one launch (start us, length us, event | category | flops | bytes accessed | tf_op | source)
XLA Modules:
  0.0 162.4 jit_solution(9880769183734100166)
XLA Ops:
  0.0 1.7 %shard_map.73 = bf16[2,64,256]{2,1,0:T(8,128)(2,1)} custom-call(bf16[2,64,64]{2,1,0:T(8,128)(2,1)} %refs_0_.1, bf16[2,64,64]{2,1,0:T(8,128)(2,1)} %refs_1_.1, bf16[2,64,64]{2,1,0:T(8,128)(2,1)} %refs_2_.1, bf16[2,16,256]{2,1,0:T(8,128)(2,1)} %refs_3_.1), custom_call_target="tpu_custom_call" | custom-call | tf_op jit(solution)/shard_map/pallas_call | solution.py:41
  1.8 53.0 %all_gather.3 = bf16[1024,256]{1,0:T(8,128)(2,1)S(1)} all-gather(bf16[128,256]{1,0:T(8,128)(2,1)} %bitcast.13), channel_id=1, replica_groups={{0,128,256,384,512,640,768,896},{16,144,272,400,528,656,784,912},{32,16..., dimensions={0}, use_global_device_ids=true | all-gather | bytes 589824 | tf_op jit(solution)/shard_map/all_gather | solution.py:207
  54.7 9.0 %collective-permute-start = (bf16[1024,256]{1,0:T(8,128)(2,1)S(1)}, bf16[1024,256]{1,0:T(8,128)(2,1)S(1)}, u32[]{:S(2)}, u32[]{:S(2)}) collective-permute-start(bf16[1024,256]{1,0:T(8,128)(2,1)S(1)} %all_gather.3), channel_id=1, source_target_pairs={{0,16},{16,0},{32,48},{48,32},{64,80},{80,64},{96,112},{112,96},{1... | collective-permute-start | bytes 1572872 | tf_op jit(solution)/shard_map/ppermute | solution.py:201
  65.4 2.8 %collective-permute-start.1 = (bf16[1024,256]{1,0:T(8,128)(2,1)S(1)}, bf16[1024,256]{1,0:T(8,128)(2,1)}, u32[]{:S(2)}, u32[]{:S(2)}) collective-permute-start(bf16[1024,256]{1,0:T(8,128)(2,1)S(1)} %pad_maximum_fusion.1.own), channel_id=1, source_target_pairs={{0,32},{16,1008},{32,64},{48,16},{64,96},{80,48},{96,128},{112,80}... | collective-permute-start | bytes 1572872 | tf_op jit(solution)/shard_map/ppermute | solution.py:197
  68.2 1.9 %collective-permute-start.2 = (bf16[512,256]{1,0:T(8,128)(2,1)S(1)}, bf16[512,256]{1,0:T(8,128)(2,1)S(1)}, u32[]{:S(2)}, u32[]{:S(2)}) collective-permute-start(bf16[512,256]{1,0:T(8,128)(2,1)S(1)} %bitcast.10), channel_id=1, source_target_pairs={{0,64},{16,976},{32,96},{48,1008},{64,128},{80,16},{96,160},{112,4... | collective-permute-start | bytes 786440 | tf_op jit(solution)/shard_map/ppermute | solution.py:197
  70.7 3.2 %collective-permute-start.3 = (bf16[8,4096]{1,0:T(8,128)(2,1)}, bf16[8,4096]{1,0:T(8,128)(2,1)S(1)}, u32[]{:S(2)}, u32[]{:S(2)}) collective-permute-start(bf16[8,4096]{1,0:T(8,128)(2,1)} %slice.19), channel_id=1, source_target_pairs={{0,16},{16,32},{32,48},{48,64},{64,80},{80,96},{96,112},{112,128},... | collective-permute-start | bytes 196616 | tf_op jit(solution)/shard_map/ppermute | solution.py:224
  74.0 2.2 %collective-permute-done.3.before = bf16[8,4096]{1,0:T(8,128)(2,1)S(1)} collective-permute-done((bf16[8,4096]{1,0:T(8,128)(2,1)}, bf16[8,4096]{1,0:T(8,128)(2,1)S(1)}, u32[]{:S(2)}, u32[]{:S(2)}) %collective-permute-start.3) | collective-permute-done | bytes 65568 | tf_op jit(solution)/shard_map/ppermute | solution.py:224
  76.9 6.0 %collective-permute-done.2 = bf16[512,256]{1,0:T(8,128)(2,1)S(1)} collective-permute-done((bf16[512,256]{1,0:T(8,128)(2,1)S(1)}, bf16[512,256]{1,0:T(8,128)(2,1)S(1)}, u32[]{:S(2)}, u32[]{:S(2)}) %collective-permute-start.2) | collective-permute-done | bytes 262176 | tf_op jit(solution)/shard_map/ppermute | solution.py:197
  84.0 2.8 %collective-permute-start.4 = (bf16[1536,256]{1,0:T(8,128)(2,1)S(1)}, bf16[1536,256]{1,0:T(8,128)(2,1)S(1)}, u32[]{:S(2)}, u32[]{:S(2)}) collective-permute-start(bf16[1536,256]{1,0:T(8,128)(2,1)S(1)} %pad_maximum_fusion.near), channel_id=1, source_target_pairs={{0,16},{16,0},{32,48},{48,32},{64,80},{80,64},{96,112},{112,96},{1... | collective-permute-start | bytes 2359304 | tf_op jit(solution)/shard_map/ppermute | solution.py:201
  86.8 1.9 %collective-permute-done.4.near_far = bf16[1536,256]{1,0:T(8,128)(2,1)S(1)} collective-permute-done((bf16[1536,256]{1,0:T(8,128)(2,1)S(1)}, bf16[1536,256]{1,0:T(8,128)(2,1)S(1)}, u32[]{:S(2)}, u32[]{:S(2)}) %collective-permute-start.4) | collective-permute-done | bytes 786464 | tf_op jit(solution)/shard_map/ppermute | solution.py:201
  88.7 1.6 shard_map.74
  90.3 16.5 %all_to_all.15.gathered = bf16[16,136,128]{2,1,0:T(8,128)(2,1)} all-to-all(bf16[16,136,128]{2,1,0:T(8,128)(2,1)S(1)} %get-tuple-element.15), channel_id=1, replica_groups=mesh['sp'=64,'tp'=16] {'tp'}, dimensions={0} | all-to-all | bytes 1114112 | tf_op jit(solution)/shard_map/all_to_all | solution.py:254
  106.8 3.1 %shard_map.75 = bf16[16,264,256]{2,1,0:T(8,128)(2,1)} custom-call(bf16[16,136,128]{2,1,0:T(8,128)(2,1)} %all_to_all.15.gathered, bf16[1024,256]{1,0:T(8,128)(2,1)} %copy-done.3, bf16[264,256]{1,0:T(8,128)(2,1)} %fusion.resid), custom_call_target="tpu_custom_call" | custom-call | flops 138412032 | bytes 4194304 | tf_op jit(solution)/shard_map/pallas_call | solution.py:255
  109.9 3.7 %all-to-all-start.1 = ((bf16[16,264,256]{2,1,0:T(8,128)(2,1)}), bf16[16,264,256]{2,1,0:T(8,128)(2,1)S(1)}, u32[]{:S(2)}, u32[]{:S(2)}) async-start(bf16[16,264,256]{2,1,0:T(8,128)(2,1)} %shard_map.75), calls=%async_computation.1 | async-start | bytes 4325376 | tf_op jit(solution)/shard_map/all_to_all | solution.py:269
  114.6 1.9 %collective-permute-start.5 = (bf16[1024,256]{1,0:T(8,128)(2,1)S(1)}, bf16[1024,256]{1,0:T(8,128)(2,1)S(1)}, u32[]{:S(2)}, u32[]{:S(2)}) collective-permute-start(bf16[1024,256]{1,0:T(8,128)(2,1)S(1)} %pad_maximum_fusion.2.own), channel_id=1, source_target_pairs={{0,32},{16,1008},{32,64},{48,16},{64,96},{80,48},{96,128},{112,80}... | collective-permute-start | bytes 1572872 | tf_op jit(solution)/shard_map/ppermute | solution.py:197
  116.5 5.6 %collective-permute-start.6 = (bf16[512,256]{1,0:T(8,128)(2,1)}, bf16[512,256]{1,0:T(8,128)(2,1)S(1)}, u32[]{:S(2)}, u32[]{:S(2)}) collective-permute-start(bf16[512,256]{1,0:T(8,128)(2,1)} %bitcast.5), channel_id=1, source_target_pairs={{0,64},{16,976},{32,96},{48,1008},{64,128},{80,16},{96,160},{112,4... | collective-permute-start | bytes 786440 | tf_op jit(solution)/shard_map/ppermute | solution.py:197
  122.1 2.7 %collective-permute-done.5 = bf16[1024,256]{1,0:T(8,128)(2,1)S(1)} collective-permute-done((bf16[1024,256]{1,0:T(8,128)(2,1)S(1)}, bf16[1024,256]{1,0:T(8,128)(2,1)S(1)}, u32[]{:S(2)}, u32[]{:S(2)}) %collective-permute-start.5) | collective-permute-done | bytes 524320 | tf_op jit(solution)/shard_map/ppermute | solution.py:197
  124.9 5.2 %collective-permute-done.6 = bf16[512,256]{1,0:T(8,128)(2,1)S(1)} collective-permute-done((bf16[512,256]{1,0:T(8,128)(2,1)}, bf16[512,256]{1,0:T(8,128)(2,1)S(1)}, u32[]{:S(2)}, u32[]{:S(2)}) %collective-permute-start.6) | collective-permute-done | bytes 262176 | tf_op jit(solution)/shard_map/ppermute | solution.py:197
  130.1 3.4 %collective-permute-start.7 = (bf16[1536,256]{1,0:T(8,128)(2,1)S(1)}, bf16[1536,256]{1,0:T(8,128)(2,1)S(1)}, u32[]{:S(2)}, u32[]{:S(2)}) collective-permute-start(bf16[1536,256]{1,0:T(8,128)(2,1)S(1)} %constant_dynamic-update-slice_fusion.near), channel_id=1, source_target_pairs={{0,16},{16,0},{32,48},{48,32},{64,80},{80,64},{96,112},{112,96},{1... | collective-permute-start | bytes 2359304 | tf_op jit(solution)/shard_map/ppermute | solution.py:201
  133.5 1.9 %collective-permute-done.7.near_far = bf16[1536,256]{1,0:T(8,128)(2,1)S(1)} collective-permute-done((bf16[1536,256]{1,0:T(8,128)(2,1)S(1)}, bf16[1536,256]{1,0:T(8,128)(2,1)S(1)}, u32[]{:S(2)}, u32[]{:S(2)}) %collective-permute-start.7) | collective-permute-done | bytes 786464 | tf_op jit(solution)/shard_map/ppermute | solution.py:201
  136.3 6.4 %all-to-all-done.1.x = bf16[16,264,256]{2,1,0:T(8,128)(2,1)S(1)} async-done(((bf16[16,264,256]{2,1,0:T(8,128)(2,1)}), bf16[16,264,256]{2,1,0:T(8,128)(2,1)S(1)}, u32[]{:S(2)}, u32[]{:S(2)}) %all-to-all-start.1) | async-done | bytes 2162720 | tf_op jit(solution)/shard_map/all_to_all | solution.py:269
  142.6 1.1 copy-done.2
  143.8 1.6 shard_map.76
  145.4 16.0 %all_to_all.16.gathered = bf16[16,128,128]{2,1,0:T(8,128)(2,1)S(1)} all-to-all(bf16[16,128,128]{2,1,0:T(8,128)(2,1)S(1)} %get-tuple-element.18), channel_id=1, replica_groups=mesh['sp'=64,'tp'=16] {'tp'}, dimensions={0} | all-to-all | bytes 1048576 | tf_op jit(solution)/shard_map/all_to_all | solution.py:279
  (24 shorter events, 7.0 us)
Async XLA Ops:
  0.0 70.1 %copy-start = (bf16[256,4096]{1,0:T(8,128)(2,1)S(1)}, bf16[256,4096]{1,0:T(8,128)(2,1)}, u32[]{:S(2)}) copy-start(bf16[256,4096]{1,0:T(8,128)(2,1)} %x.1) | copy-start | bytes 6291460
  54.7 10.6 %collective-permute-start = (bf16[1024,256]{1,0:T(8,128)(2,1)S(1)}, bf16[1024,256]{1,0:T(8,128)(2,1)S(1)}, u32[]{:S(2)}, u32[]{:S(2)}) collective-permute-start(bf16[1024,256]{1,0:T(8,128)(2,1)S(1)} %all_gather.3), channel_id=1, source_target_pairs={{0,16},{16,0},{32,48},{48,32},{64,80},{80,64},{96,112},{112,96},{1... | collective-permute-start | bytes 1572872 | tf_op jit(solution)/shard_map/ppermute | solution.py:201
  65.4 21.4 %copy-start.5 = (f32[2,3,64]{2,0,1:T(2,128)S(1)}, f32[2,3,64]{2,0,1:T(2,128)}, u32[]{:S(2)}) copy-start(f32[2,3,64]{2,0,1:T(2,128)} %param.13) | copy-start | bytes 4612
  65.4 23.3 %copy-start.4 = (f32[2,4096]{1,0:T(2,128)S(1)}, f32[2,4096]{1,0:T(2,128)}, u32[]{:S(2)}) copy-start(f32[2,4096]{1,0:T(2,128)} %gain.3) | copy-start | bytes 98308
  65.4 17.5 %collective-permute-start.1 = (bf16[1024,256]{1,0:T(8,128)(2,1)S(1)}, bf16[1024,256]{1,0:T(8,128)(2,1)}, u32[]{:S(2)}, u32[]{:S(2)}) collective-permute-start(bf16[1024,256]{1,0:T(8,128)(2,1)S(1)} %pad_maximum_fusion.1.own), channel_id=1, source_target_pairs={{0,32},{16,1008},{32,64},{48,16},{64,96},{80,48},{96,128},{112,80}... | collective-permute-start | bytes 1572872 | tf_op jit(solution)/shard_map/ppermute | solution.py:197
  68.2 14.7 %collective-permute-start.2 = (bf16[512,256]{1,0:T(8,128)(2,1)S(1)}, bf16[512,256]{1,0:T(8,128)(2,1)S(1)}, u32[]{:S(2)}, u32[]{:S(2)}) collective-permute-start(bf16[512,256]{1,0:T(8,128)(2,1)S(1)} %bitcast.10), channel_id=1, source_target_pairs={{0,64},{16,976},{32,96},{48,1008},{64,128},{80,16},{96,160},{112,4... | collective-permute-start | bytes 786440 | tf_op jit(solution)/shard_map/ppermute | solution.py:197
  70.7 5.4 %collective-permute-start.3 = (bf16[8,4096]{1,0:T(8,128)(2,1)}, bf16[8,4096]{1,0:T(8,128)(2,1)S(1)}, u32[]{:S(2)}, u32[]{:S(2)}) collective-permute-start(bf16[8,4096]{1,0:T(8,128)(2,1)} %slice.19), channel_id=1, source_target_pairs={{0,16},{16,32},{32,48},{48,64},{64,80},{80,96},{96,112},{112,128},... | collective-permute-start | bytes 196616 | tf_op jit(solution)/shard_map/ppermute | solution.py:224
  84.0 4.7 %collective-permute-start.4 = (bf16[1536,256]{1,0:T(8,128)(2,1)S(1)}, bf16[1536,256]{1,0:T(8,128)(2,1)S(1)}, u32[]{:S(2)}, u32[]{:S(2)}) collective-permute-start(bf16[1536,256]{1,0:T(8,128)(2,1)S(1)} %pad_maximum_fusion.near), channel_id=1, source_target_pairs={{0,16},{16,0},{32,48},{48,32},{64,80},{80,64},{96,112},{112,96},{1... | collective-permute-start | bytes 2359304 | tf_op jit(solution)/shard_map/ppermute | solution.py:201
  90.3 16.5 %copy-start.3 = (bf16[1024,256]{1,0:T(8,128)(2,1)}, bf16[1024,256]{1,0:T(8,128)(2,1)S(1)}, u32[]{:S(2)}) copy-start(bf16[1024,256]{1,0:T(8,128)(2,1)S(1)} %get-tuple-element.16.wb) | copy-start | bytes 1572868
  109.9 32.8 %all-to-all-start.1 = ((bf16[16,264,256]{2,1,0:T(8,128)(2,1)}), bf16[16,264,256]{2,1,0:T(8,128)(2,1)S(1)}, u32[]{:S(2)}, u32[]{:S(2)}) async-start(bf16[16,264,256]{2,1,0:T(8,128)(2,1)} %shard_map.75), calls=%async_computation.1 | async-start | bytes 4325376 | tf_op jit(solution)/shard_map/all_to_all | solution.py:269
  114.6 10.2 %collective-permute-start.5 = (bf16[1024,256]{1,0:T(8,128)(2,1)S(1)}, bf16[1024,256]{1,0:T(8,128)(2,1)S(1)}, u32[]{:S(2)}, u32[]{:S(2)}) collective-permute-start(bf16[1024,256]{1,0:T(8,128)(2,1)S(1)} %pad_maximum_fusion.2.own), channel_id=1, source_target_pairs={{0,32},{16,1008},{32,64},{48,16},{64,96},{80,48},{96,128},{112,80}... | collective-permute-start | bytes 1572872 | tf_op jit(solution)/shard_map/ppermute | solution.py:197
  116.5 13.5 %collective-permute-start.6 = (bf16[512,256]{1,0:T(8,128)(2,1)}, bf16[512,256]{1,0:T(8,128)(2,1)S(1)}, u32[]{:S(2)}, u32[]{:S(2)}) collective-permute-start(bf16[512,256]{1,0:T(8,128)(2,1)} %bitcast.5), channel_id=1, source_target_pairs={{0,64},{16,976},{32,96},{48,1008},{64,128},{80,16},{96,160},{112,4... | collective-permute-start | bytes 786440 | tf_op jit(solution)/shard_map/ppermute | solution.py:197
  130.1 5.3 %collective-permute-start.7 = (bf16[1536,256]{1,0:T(8,128)(2,1)S(1)}, bf16[1536,256]{1,0:T(8,128)(2,1)S(1)}, u32[]{:S(2)}, u32[]{:S(2)}) collective-permute-start(bf16[1536,256]{1,0:T(8,128)(2,1)S(1)} %constant_dynamic-update-slice_fusion.near), channel_id=1, source_target_pairs={{0,16},{16,0},{32,48},{48,32},{64,80},{80,64},{96,112},{112,96},{1... | collective-permute-start | bytes 2359304 | tf_op jit(solution)/shard_map/ppermute | solution.py:201
  135.4 0.9 copy-start.1
  142.6 1.1 copy-start.2
